TPU v7x, 128 devices: a whole 4x4x4 slice. The times are simulated.
128 devices in a mesh: sp: 16 (over z, y), tp: 8 (over x, core).
Axes of the slice: x: 4, y: 4, z: 4, core: 2. Of those that a mesh axis runs over, the one named last changes fastest.
Arguments:
- layer_input_rows: bfloat16 [4096, 2048], P('sp'), may hold values from -6 to 6
- input_norm_gain: float32 [2048], replicated, may hold values from 0.1 to 1.9
- query_weight: bfloat16 [2048, 1024], P(None, 'tp'), may hold values from -0.125 to 0.125
- key_weight: bfloat16 [2048, 1024], P(None, 'tp'), may hold values from -0.125 to 0.125
- value_weight: bfloat16 [2048, 1024], P(None, 'tp'), may hold values from -0.125 to 0.125
- query_norm_gain: float32 [64], replicated, may hold values from 0.5 to 9
- key_norm_gain: float32 [64], replicated, may hold values from 0.5 to 9
- cumulative_gate: float32 [4096, 16], P('sp', 'tp'), may hold values from -575.44 to 0, as said below
- attention_norm_gain: float32 [1024], P('tp'), may hold values from 0.1 to 1.9
- recurrence_query_weight: bfloat16 [2048, 1024], P(None, 'tp'), may hold values from -0.125 to 0.125
- forget_weight: bfloat16 [2048, 1024], P(None, 'tp'), may hold values from -0.125 to 0.125
- recurrence_value_weight: bfloat16 [2048, 1024], P(None, 'tp'), may hold values from -0.125 to 0.125
- output_gate_weight: bfloat16 [2048, 1024], P(None, 'tp'), may hold values from -0.125 to 0.125
- gate_lower_slack: float32 [1024], P('tp'), may hold values from 0 to 0.06
- extra_log_decay: float32 [4096, 8], P('sp', 'tp'), may hold values from -1.5 to 0
- recurrence_norm_gain: float32 [1024], P('tp'), may hold values from 0.1 to 1.9
- attention_output_weight: bfloat16 [1024, 2048], P('tp'), may hold values from -0.125 to 0.125
- recurrence_output_weight: bfloat16 [1024, 2048], P('tp'), may hold values from -0.125 to 0.125
Outputs:
- mixed: bfloat16 [4096, 2048], P(('sp', 'tp'))
- log_sum: float32 [4096, 16], P('sp', 'tp')
Inputs may be any that keep to these rules, and one draw needn't show every extreme that they name: `cumulative_gate`: each column never rises along positions.
All inputs are finite; a program needn't handle non-finite values.
Results may differ from a plain program's by a relative error of at most 0.015.
The roundings to bfloat16 on the way count: a program that leaves them out, or rounds other values in their place, can miss the bound.
Values may be sent and summed in bfloat16 or wider, within the bound.
A program may use at most 64 MiB of HBM per device.

v0:
```python
import math

import jax
import jax.numpy as jnp
from jax import lax
from jax.sharding import Mesh
from jax.sharding import PartitionSpec as P

HEAD_DIM = 64
STATE_ROWS = 128
VAL_DIM = 128
BLOCK = 64
SP = ("sp_0", "sp_1")
SP_TP = ("sp_0", "sp_1", "tp")


EPSILON = 1e-06


def from_everyone(shard, axis):
    count = lax.axis_size(axis)
    return lax.all_to_all(
        jnp.broadcast_to(shard[None], (count, *shard.shape)), axis, 0, 0, tiled=True
    )


def joined_along(parts, dim):
    parts = jnp.moveaxis(parts, 0, dim)
    lengths = parts.shape
    return parts.reshape(*lengths[:dim], lengths[dim] * lengths[dim + 1], *lengths[dim + 2 :])


def gather_directly(shard, axis, dim):
    parts = from_everyone(shard, axis)
    return joined_along(parts, dim)


def sent_together(arrays, axis, dim, along):
    both = jnp.concatenate(arrays, axis=along)
    whole, at, finished = (lax.all_gather(both, axis, axis=dim, tiled=True), 0, [])
    for a in arrays:
        finished.append(lax.slice_in_dim(whole, at, at + a.shape[along], axis=along))
        at += a.shape[along]
    return tuple(finished)


def nothing_yet(shard, identity):
    return jax.tree.map(
        lambda a, e: jnp.broadcast_to(jnp.asarray(e, a.dtype), a.shape), shard, identity
    )


def collected_together(shard, axis):
    leaves = jax.tree.leaves(shard)
    order = sorted(range(len(leaves)), key=lambda k: -leaves[k].size)
    width = (1, *leaves[order[0]].shape)[-1]
    lines = [
        jnp.pad(leaves[k].reshape(-1), (0, -leaves[k].size % width)).reshape(-1, width)
        for k in order
    ]
    both, at, found = (lax.all_gather(jnp.concatenate(lines), axis), 0, {})
    for k, line in zip(order, lines):
        share = both[:, at : at + len(line)].reshape(len(both), -1)
        found[k] = share[:, : leaves[k].size].reshape(-1, *leaves[k].shape)
        at += len(line)
    numbers = iter(range(len(leaves)))
    return jax.tree.map(lambda _: found[next(numbers)], shard)


def carried_in(shard, axes, combine, identity):
    before = start = nothing_yet(shard, identity)
    total = shard
    for axis in reversed(axes):
        count, index = (lax.axis_size(axis), lax.axis_index(axis))
        pieces = collected_together(
            jax.tree.map(lambda part, kind: part.astype(kind), total, (jnp.bfloat16, jnp.bfloat16)),
            axis,
        )
        inside, total = (start, start)
        for k in range(count):
            passed = k < index
            total = combine(
                total, jax.tree.map(lambda part, own: part[k].astype(own.dtype), pieces, shard)
            )
            inside = jax.tree.map(lambda new, old: jnp.where(passed, new, old), total, inside)
        before = combine(inside, before)
    return before


def in_blocks(shard, dim, count):
    before, after = (shard.shape[:dim], shard.shape[dim + 1 :])
    return jnp.moveaxis(shard.reshape(*before, count, -1, *after), dim, 0)


def sum_at_owner(shard, axis, dim):
    parts = in_blocks(shard, dim, lax.axis_size(axis))
    arrived = lax.all_to_all(parts, axis, split_axis=0, concat_axis=0, tiled=True)
    return arrived.astype(jnp.float32).sum(axis=0)


def rms_rows(values, gain):
    squares = jnp.mean(values * values, axis=-1, keepdims=True)
    return values * lax.rsqrt(squares + EPSILON) * gain


def project(normalized_input, weight):
    return jnp.dot(normalized_input, weight, preferred_element_type=jnp.float32)


def recur_blocks(rec_query, forget_fraction, rec_value, decay_logarithm, states):
    length, head_number, keydim = rec_query.shape
    span_rows = BLOCK
    blocks = length // span_rows
    lower_tri = jnp.arange(span_rows)[:, None] >= jnp.arange(span_rows)[None, :]

    def to_blocks(values):
        return values.reshape(blocks, span_rows, head_number, values.shape[-1])

    def recur_advance(carried, inputs):
        current_states, running = carried
        query_block, share_block, value_block, decay_blk = inputs
        within_block = jnp.cumsum(decay_blk, axis=0)
        differ = within_block[:, None] - within_block[None, :]
        fading = jnp.exp(jnp.where(lower_tri[:, :, None, None], differ, -jnp.inf))
        scores = jnp.einsum("thk,tshk,shk->tsh", query_block, fading, share_block)
        inner_part = jnp.einsum("tsh,shv->thv", scores, value_block)
        carried_piece = jnp.einsum(
            "zbf,bfw->zbw", query_block * jnp.exp(within_block), current_states
        )
        closing_state = within_block[-1]
        current_states = jnp.exp(closing_state)[:, :, None] * current_states + jnp.einsum(
            "tfo,tfw->fow", share_block * jnp.exp(closing_state[None] - within_block), value_block
        )
        visible_query = query_block * jnp.exp(running[None] + within_block)
        return (
            (current_states, running + closing_state),
            (inner_part + carried_piece, visible_query),
        )

    zeros_run = jnp.zeros((head_number, keydim), jnp.float32)
    (states, running), (outputs, visible_query) = lax.scan(
        recur_advance,
        (states, zeros_run),
        (
            to_blocks(rec_query),
            to_blocks(forget_fraction),
            to_blocks(rec_value),
            to_blocks(decay_logarithm),
        ),
    )
    return (
        outputs.reshape(length, head_number, -1),
        states,
        running,
        visible_query.reshape(length, head_number, keydim),
    )


def attend(
    normalized_input,
    query_weight,
    key_weight,
    value_weight,
    query_norm_gain,
    key_norm_gain,
    cumulative_gate,
    attention_norm_gain,
):
    token_rows = normalized_input.shape[0]
    att_local = query_weight.shape[1] // HEAD_DIM
    sp_index = lax.axis_index(SP)
    queries = rms_rows(
        project(normalized_input, query_weight).reshape(token_rows, att_local, HEAD_DIM),
        query_norm_gain,
    )
    queries = queries.astype(jnp.bfloat16)
    keys = rms_rows(
        project(normalized_input, key_weight).reshape(token_rows, att_local, HEAD_DIM),
        key_norm_gain,
    )
    keys = keys.astype(jnp.bfloat16).reshape(token_rows, att_local * HEAD_DIM)
    values = project(normalized_input, value_weight).astype(jnp.bfloat16)
    all_cum = gather_directly(cumulative_gate, SP, 0)
    query_pos = sp_index * token_rows + jnp.arange(token_rows, dtype=jnp.int32)
    query_cum = cumulative_gate.T
    score_scale = HEAD_DIM ** (-0.5)

    def absorb(carried, key_blk, value_block, offset):
        row_top, totals, sums = carried
        width = key_blk.shape[0]
        key_heads = key_blk.reshape(width, att_local, HEAD_DIM)
        value_heads = value_block.reshape(width, att_local, HEAD_DIM)
        key_cum = lax.dynamic_slice_in_dim(all_cum, offset, width, 0).T
        scores = (
            jnp.einsum("qhd,khd->hqk", queries, key_heads, preferred_element_type=jnp.float32)
            * score_scale
        )
        scores = scores + query_cum[:, :, None] - key_cum[:, None, :]
        key_pos = offset + jnp.arange(width, dtype=jnp.int32)
        causal = key_pos[None, :] <= query_pos[:, None]
        scores = jnp.where(causal[None], scores, -jnp.inf)
        new_top = jnp.maximum(row_top, jnp.max(scores, axis=-1))
        anchor = jnp.where(jnp.isfinite(new_top), new_top, 0.0)
        weights = jnp.exp(scores - anchor[:, :, None])
        fading = jnp.exp(row_top - anchor)
        totals = totals * fading + jnp.sum(weights, axis=-1)
        sums = sums * fading[:, :, None] + jnp.einsum(
            "hqk,khd->hqd",
            weights.astype(jnp.bfloat16),
            value_heads,
            preferred_element_type=jnp.float32,
        )
        return (new_top, totals, sums)

    start_carry = (
        jnp.full((att_local, token_rows), -jnp.inf, jnp.float32),
        jnp.zeros((att_local, token_rows), jnp.float32),
        jnp.zeros((att_local, token_rows, HEAD_DIM), jnp.float32),
    )
    carried = start_carry
    key_rows, value_rows = sent_together((keys, values), SP, 0, 1)
    length = key_rows.shape[0]
    width = math.gcd(length, 512)

    def fold_advance(inner_carry, block_index):
        begin = block_index * width
        key_blk = lax.dynamic_slice_in_dim(key_rows, begin, width, 0)
        value_block = lax.dynamic_slice_in_dim(value_rows, begin, width, 0)
        return (absorb(inner_carry, key_blk, value_block, begin), None)

    carried, ignored = lax.scan(fold_advance, carried, jnp.arange(length // width, dtype=jnp.int32))
    row_top, totals, sums = carried
    attention = (sums / totals[:, :, None]).transpose(1, 0, 2)
    attn_out = rms_rows(attention, attention_norm_gain.reshape(att_local, HEAD_DIM)).astype(
        jnp.bfloat16
    )
    log_sum = (row_top + jnp.log(totals)).T
    return (attn_out.reshape(token_rows, att_local * HEAD_DIM), log_sum)


def recurrence_result(
    normalized_input,
    recurrence_query_weight,
    forget_weight,
    recurrence_value_weight,
    output_gate_weight,
    gate_lower_slack,
    extra_log_decay,
    recurrence_norm_gain,
):
    token_rows = normalized_input.shape[0]
    recurrence_local = recurrence_query_weight.shape[1] // STATE_ROWS
    rec_query = jax.nn.silu(project(normalized_input, recurrence_query_weight)).reshape(
        token_rows, recurrence_local, STATE_ROWS
    )
    forget_fraction = gate_lower_slack * jax.nn.sigmoid(-project(normalized_input, forget_weight))
    decay_logarithm = (
        jnp.log1p(-forget_fraction).reshape(token_rows, recurrence_local, STATE_ROWS)
        + extra_log_decay[:, :, None]
    )
    rec_value = lax.optimization_barrier(
        project(normalized_input, recurrence_value_weight).astype(jnp.bfloat16)
    ).astype(jnp.float32)
    rec_value = rec_value.reshape(token_rows, recurrence_local, VAL_DIM)
    start_states = jnp.zeros((recurrence_local, STATE_ROWS, VAL_DIM), jnp.float32)
    local_output, final_states, run_total, visible_query = recur_blocks(
        rec_query,
        forget_fraction.reshape(token_rows, recurrence_local, STATE_ROWS),
        rec_value,
        decay_logarithm,
        start_states,
    )

    def chain(earlier, later):
        return (earlier[0] + later[0], jnp.exp(later[0])[:, :, None] * earlier[1] + later[1])

    identity = (jnp.zeros_like(run_total), jnp.zeros_like(final_states))
    incoming_state = carried_in((run_total, final_states), SP, chain, identity)[1]
    recurrent_output = local_output + jnp.einsum("zbf,bfw->zbw", visible_query, incoming_state)
    out_gate = jax.nn.silu(project(normalized_input, output_gate_weight)).reshape(
        token_rows, recurrence_local, VAL_DIM
    )
    rec_out = (
        rms_rows(recurrent_output, recurrence_norm_gain.reshape(recurrence_local, VAL_DIM))
        * out_gate
    )
    return rec_out.astype(jnp.bfloat16).reshape(token_rows, recurrence_local * VAL_DIM)


def body(
    layer_input_rows,
    input_norm_gain,
    query_weight,
    key_weight,
    value_weight,
    query_norm_gain,
    key_norm_gain,
    cumulative_gate,
    attention_norm_gain,
    recurrence_query_weight,
    forget_weight,
    recurrence_value_weight,
    output_gate_weight,
    gate_lower_slack,
    extra_log_decay,
    recurrence_norm_gain,
    attention_output_weight,
    recurrence_output_weight,
):
    normalized_input = rms_rows(layer_input_rows.astype(jnp.float32), input_norm_gain).astype(
        jnp.bfloat16
    )
    attn_out, log_sum = attend(
        normalized_input,
        query_weight,
        key_weight,
        value_weight,
        query_norm_gain,
        key_norm_gain,
        cumulative_gate,
        attention_norm_gain,
    )
    rec_out = recurrence_result(
        normalized_input,
        recurrence_query_weight,
        forget_weight,
        recurrence_value_weight,
        output_gate_weight,
        gate_lower_slack,
        extra_log_decay,
        recurrence_norm_gain,
    )
    summed = jnp.dot(attn_out, attention_output_weight, preferred_element_type=jnp.float32)
    mixed_rows = sum_at_owner(
        (
            summed + jnp.dot(rec_out, recurrence_output_weight, preferred_element_type=jnp.float32)
        ).astype(jnp.bfloat16),
        "tp",
        0,
    ).astype(jnp.bfloat16)
    return (mixed_rows, log_sum)


def solution(mesh):
    finer = Mesh(mesh.devices.reshape(4, 4, mesh.shape["tp"]), ("sp_0", "sp_1", "tp"))
    placed = (
        P(SP, None),
        P(),
        P(None, "tp"),
        P(None, "tp"),
        P(None, "tp"),
        P(),
        P(),
        P(SP, "tp"),
        P("tp"),
        P(None, "tp"),
        P(None, "tp"),
        P(None, "tp"),
        P(None, "tp"),
        P("tp"),
        P(SP, "tp"),
        P("tp"),
        P("tp", None),
        P("tp", None),
    )
    return jax.shard_map(
        body, mesh=finer, in_specs=placed, out_specs=(P(SP_TP, None), P(SP, "tp")), check_vma=False
    )
```

profile of v0, /device:TPU:1, one launch (start us, length us, event | category | flops | bytes accessed | tf_op | source)
XLA Modules:
  0.0 126.8 jit_solution(18322435534652590707)
XLA Ops:
  7.2 1.6 %fusion.48 = f32[256]{0:T(256)S(1)} fusion(bf16[256,2048]{1,0:T(8,128)(2,1)} %param.22), kind=kLoop, calls=%fused_computation.73 | loop fusion | flops 1572608 | bytes 1049600 | tf_op jit(solution)/shard_map/reduce_sum | solution.py:102
  8.9 1.6 %fusion.50 = bf16[256,2048]{1,0:T(8,128)(2,1)S(1)} fusion(bf16[256,2048]{1,0:T(8,128)(2,1)} %param.22, f32[2048]{0:T(1024)} %param.23, f32[256]{0:T(256)S(1)} %add_rsqrt_fusion.4), kind=kLoop, calls=%fused_computation.75 | loop fusion | flops 2097152 | bytes 2106368 | tf_op jit(solution)/shard_map/convert_element_type | solution.py:310
  10.5 0.5 bitcast_reduce_fusion
  11.1 0.5 convolution_convert_fusion.1
  11.7 0.7 pad_maximum_fusion
  12.4 0.6 broadcast_in_dim.46
  13.0 8.6 %all-to-all-start = ((f32[16,256,2]{1,2,0:T(2,128)}), f32[16,256,2]{1,2,0:T(2,128)S(1)}, u32[]{:S(2)}, u32[]{:S(2)}) async-start(f32[16,256,2]{1,2,0:T(2,128)} %broadcast_in_dim.46), calls=%async_computation | async-start | bytes 65536 | tf_op jit(solution)/shard_map/all_to_all | solution.py:22
  21.7 0.4 convolution_convert_fusion
  22.1 1.5 %divide_multiply_fusion = f32[256,128]{1,0:T(8,128)S(1)} fusion(bf16[256,2048]{1,0:T(8,128)(2,1)S(1)} %fusion.50, bf16[2048,128]{1,0:T(8,128)(2,1)} %param.31), kind=kOutput, calls=%fused_computation.97 | convolution fusion | flops 134348800 | bytes 1703936 | tf_op jit(solution)/shard_map/dot_general | solution.py:107
  23.6 0.5 log-plus-one_add_fusion
  24.1 6.5 %while.33 = (s32[]{:T(128)}, f32[1,128,128]{2,1,0:T(8,128)S(1)}, f32[1,128]{1,0:T(1,128)S(1)}, f32[4,64,1,128]{3,1,2,0:T(8,128)S(1)}, bf16[4,64,1,128]{3,1,2,0:T...) while((s32[]{:T(128)}, f32[1,128,128]{2,1,0:T(8,128)S(1)}, ...), condition=%wide.region_10.11_spmd.clone, body=%wide.region_8.10_spmd.clone.sunk | while | flops 8499459 | bytes 1030797 | solution.py:141
  24.3 0.9 fusion.206
  25.5 0.2 fusion.204
  25.9 0.9 fusion.206
  27.2 0.2 fusion.204
  27.6 0.9 fusion.206
  28.8 0.2 fusion.204
  29.2 0.9 fusion.206
  30.4 0.2 fusion.204
  30.8 10.2 %all-gather.2 = bf16[4,129,128]{2,1,0:T(8,128)(2,1)S(1)} all-gather(bf16[1,129,128]{2,1,0:T(8,128)(2,1)S(1)} %maximum_bitcast_fusion), channel_id=2, replica_groups=mesh['sp_0'=4,'sp_1'=4,'tp'=8] {'sp_1'}, dimensions={0}, use_global_device_ids=true | all-gather | bytes 165120 | tf_op jit(solution)/shard_map/all_gather | solution.py:61
  41.2 9.8 %all-gather.3 = bf16[4,129,128]{2,1,0:T(8,128)(2,1)S(1)} all-gather(bf16[1,129,128]{2,1,0:T(8,128)(2,1)S(1)} %maximum_bitcast_fusion.1), channel_id=3, replica_groups=mesh['sp_0'=4,'sp_1'=4,'tp'=8] {'sp_0'}, dimensions={0}, use_global_device_ids=true | all-gather | bytes 165120 | tf_op jit(solution)/shard_map/all_gather | solution.py:61
  50.9 0.5 multiply_reduce_fusion
  51.4 0.5 multiply_reduce_fusion.1
  52.0 9.6 %all-gather.6.cloned.1.call-done = bf16[4096,256]{0,1:T(8,128)(2,1)} async-done(((bf16[256,256]{0,1:T(8,128)(2,1)}), bf16[4096,256]{0,1:T(8,128)(2,1)}) %all-gather.6.cloned.1.call-update) | async-done | bytes 2097168 | tf_op jit(solution)/shard_map/all_gather | solution.py:40
  61.7 3.1 %fusion.131 = (bf16[4096,128]{0,1:T(8,128)(2,1)}, bf16[4096,128]{0,1:T(8,128)(2,1)}) fusion(bf16[4096,256]{0,1:T(8,128)(2,1)} %all-gather.6.cloned.1.call-done), kind=kLoop, calls=%fused_computation.201 | loop fusion | bytes 4194304 | tf_op jit(solution)/shard_map/slice | solution.py:42
  64.8 27.3 %while.32 = (s32[]{:T(128)}, f32[2,256]{1,0:T(2,128)S(1)}, f32[2,256]{1,0:T(2,128)S(1)}, f32[2,256,64]{1,2,0:T(8,128)S(1)}, s32[8]{0:T(128)S(1)}, /*index=5*/bf1...) while((s32[]{:T(128)}, f32[2,256]{1,0:T(2,128)S(1)}, ...), condition=%wide.region_6.7_spmd.clone, body=%wide.region_3.6_spmd.clone.sunk | while | flops 69702912 | bytes 4577507 | solution.py:231
  64.8 0.6 dynamic_slice.61
  66.0 1.0 constant_dynamic-slice_fusion.9
  67.2 0.4 fusion.190
  67.8 0.3 convolution_add_fusion.3
  68.2 0.6 dynamic_slice.61
  69.4 1.0 constant_dynamic-slice_fusion.9
  70.6 0.4 fusion.190
  71.3 0.3 convolution_add_fusion.3
  71.6 0.6 dynamic_slice.61
  72.8 1.0 constant_dynamic-slice_fusion.9
  74.0 0.4 fusion.190
  74.7 0.3 convolution_add_fusion.3
  75.0 0.6 dynamic_slice.61
  76.3 1.0 constant_dynamic-slice_fusion.9
  77.5 0.4 fusion.190
  78.1 0.3 convolution_add_fusion.3
  78.4 0.6 dynamic_slice.61
  79.7 1.0 constant_dynamic-slice_fusion.9
  80.9 0.4 fusion.190
  81.5 0.3 convolution_add_fusion.3
  81.9 0.6 dynamic_slice.61
  83.1 1.0 constant_dynamic-slice_fusion.9
  84.3 0.4 fusion.190
  84.9 0.3 convolution_add_fusion.3
  85.3 0.6 dynamic_slice.61
  86.5 1.0 constant_dynamic-slice_fusion.9
  87.7 0.4 fusion.190
  88.3 0.3 convolution_add_fusion.3
  88.7 0.6 dynamic_slice.61
  89.9 1.0 constant_dynamic-slice_fusion.9
  91.1 0.4 fusion.190
  91.8 0.3 convolution_add_fusion.3
  92.3 1.8 %fusion.136 = f32[256,2048]{1,0:T(8,128)} fusion(bf16[256,128]{0,1:T(8,128)(2,1)S(1)} %bitcast.251, bf16[128,2048]{1,0:T(8,128)(2,1)S(1)} %copy-done), kind=kOutput, calls=%fused_computation.205 | convolution fusion | flops 134217728 | bytes 2686976 | tf_op jit(solution)/shard_map/dot_general | solution.py:333
  94.1 3.4 %fusion.47 = bf16[256,2048]{1,0:T(8,128)(2,1)} fusion(f32[256,2048]{1,0:T(8,128)} %fusion.136, bf16[128,2048]{1,0:T(8,128)(2,1)S(1)} %copy-done.3, f32[256,1,128]{2,0,1:T(8,128)S(1)} %get-tuple-element.283, f32[128]{0:T(128)S(1)} %copy-done.9, f32[256]{0:T(256)S(1)} %add_rsqrt_fusion.3, bf16[256,2048]{1,0:T(8,128)(2,1)S(1)} %fusion.50, ...), kind=kOutput, calls=%fused_computation.72 | convolution fusion | flops 269746176 | bytes 5375488 | tf_op jit(solution)/shard_map/dot_general | solution.py:336
  97.5 6.7 %all-to-all-start.1 = ((bf16[8,32,2048]{2,1,0:T(8,128)(2,1)}), bf16[8,32,2048]{2,1,0:T(8,128)(2,1)S(1)}, u32[]{:S(2)}, u32[]{:S(2)}) async-start(bf16[8,32,2048]{2,1,0:T(8,128)(2,1)} %bitcast.37), calls=%async_computation.1 | async-start | bytes 2097152 | tf_op jit(solution)/shard_map/all_to_all | solution.py:97
  104.2 0.6 add_bitcast_fusion
  104.8 14.4 %all-to-all-done.1 = bf16[8,32,2048]{2,1,0:T(8,128)(2,1)S(1)} async-done(((bf16[8,32,2048]{2,1,0:T(8,128)(2,1)}), bf16[8,32,2048]{2,1,0:T(8,128)(2,1)S(1)}, u32[]{:S(2)}, u32[]{:S(2)}) %all-to-all-start.1) | async-done | bytes 1048608 | tf_op jit(solution)/shard_map/all_to_all | solution.py:97
  119.2 0.8 reduce_sum.71
  (169 shorter events, 5.3 us)
Async XLA Ops:
  7.2 85.1 %copy-start = (bf16[128,2048]{1,0:T(8,128)(2,1)S(1)}, bf16[128,2048]{1,0:T(8,128)(2,1)}, u32[]{:S(2)}) copy-start(bf16[128,2048]{1,0:T(8,128)(2,1)} %param.38) | copy-start | bytes 1572868
  7.2 3.3 %copy-start.5 = (bf16[2048,128]{1,0:T(8,128)(2,1)S(1)}, bf16[2048,128]{1,0:T(8,128)(2,1)}, u32[]{:S(2)}) copy-start(bf16[2048,128]{1,0:T(8,128)(2,1)} %param.25) | copy-start | bytes 1572868
  7.2 54.5 %all-gather.6.cloned.1.call-start = ((), (), s32[]{:S(2)}) async-start(), calls=%async_computation.2 | async-start | bytes 2228224 | tf_op jit(solution)/shard_map/all_gather | solution.py:40
  8.8 2.2 %copy-start.12 = (f32[64]{0:T(128)S(1)}, f32[64]{0:T(128)}, u32[]{:S(2)}) copy-start(f32[64]{0:T(128)} %param.28) | copy-start | bytes 772
  8.8 2.3 %copy-start.1 = (bf16[2048,128]{1,0:T(8,128)(2,1)S(1)}, bf16[2048,128]{1,0:T(8,128)(2,1)}, u32[]{:S(2)}) copy-start(bf16[2048,128]{1,0:T(8,128)(2,1)} %param.26) | copy-start | bytes 1572868
  10.5 1.9 %copy-start.7 = (f32[256,2]{0,1:T(2,128)S(1)}, f32[256,2]{0,1:T(2,128)}, u32[]{:S(2)}) copy-start(f32[256,2]{0,1:T(2,128)} %param.29) | copy-start | bytes 6148
  10.5 11.2 %copy-start.2 = (bf16[2048,128]{1,0:T(8,128)(2,1)S(1)}, bf16[2048,128]{1,0:T(8,128)(2,1)}, u32[]{:S(2)}) copy-start(bf16[2048,128]{1,0:T(8,128)(2,1)} %param.33) | copy-start | bytes 1572868
  12.4 11.2 %copy-start.10 = (bf16[2048,128]{1,0:T(8,128)(2,1)S(1)}, bf16[2048,128]{1,0:T(8,128)(2,1)}, u32[]{:S(2)}) copy-start(bf16[2048,128]{1,0:T(8,128)(2,1)} %param.32) | copy-start | bytes 1572868
  12.4 11.2 %copy-start.11 = (f32[256,1]{0,1:T(1,128)S(1)}, f32[256,1]{0,1:T(1,128)}, u32[]{:S(2)}) copy-start(f32[256,1]{0,1:T(1,128)} %param.36) | copy-start | bytes 3076
  12.4 11.2 %copy-start.13 = (f32[128]{0:T(128)S(1)}, f32[128]{0:T(128)}, u32[]{:S(2)}) copy-start(f32[128]{0:T(128)} %param.35) | copy-start | bytes 1540
  13.0 51.7 %all-to-all-start = ((f32[16,256,2]{1,2,0:T(2,128)}), f32[16,256,2]{1,2,0:T(2,128)S(1)}, u32[]{:S(2)}, u32[]{:S(2)}) async-start(f32[16,256,2]{1,2,0:T(2,128)} %broadcast_in_dim.46), calls=%async_computation | async-start | bytes 65536 | tf_op jit(solution)/shard_map/all_to_all | solution.py:22
  24.1 6.6 %copy-start.14 = (f32[128]{0:T(128)S(1)}, f32[128]{0:T(128)}, u32[]{:S(2)}) copy-start(f32[128]{0:T(128)} %param.30) | copy-start | bytes 1540
  24.1 27.3 %copy-start.6 = (bf16[2048,128]{1,0:T(8,128)(2,1)S(1)}, bf16[2048,128]{1,0:T(8,128)(2,1)}, u32[]{:S(2)}) copy-start(bf16[2048,128]{1,0:T(8,128)(2,1)} %param.24) | copy-start | bytes 1572868
  30.6 21.3 %copy-start.8 = (f32[64]{0:T(128)S(1)}, f32[64]{0:T(128)}, u32[]{:S(2)}) copy-start(f32[64]{0:T(128)} %param.27) | copy-start | bytes 772
  92.1 2.0 %copy-start.3 = (bf16[128,2048]{1,0:T(8,128)(2,1)S(1)}, bf16[128,2048]{1,0:T(8,128)(2,1)}, u32[]{:S(2)}) copy-start(bf16[128,2048]{1,0:T(8,128)(2,1)} %param.39) | copy-start | bytes 1572868
  92.1 2.0 %copy-start.4 = (bf16[2048,128]{1,0:T(8,128)(2,1)S(1)}, bf16[2048,128]{1,0:T(8,128)(2,1)}, u32[]{:S(2)}) copy-start(bf16[2048,128]{1,0:T(8,128)(2,1)} %param.34) | copy-start | bytes 1572868
  92.1 2.0 %copy-start.9 = (f32[128]{0:T(128)S(1)}, f32[128]{0:T(128)}, u32[]{:S(2)}) copy-start(f32[128]{0:T(128)} %param.37) | copy-start | bytes 1540
  97.5 21.7 %all-to-all-start.1 = ((bf16[8,32,2048]{2,1,0:T(8,128)(2,1)}), bf16[8,32,2048]{2,1,0:T(8,128)(2,1)S(1)}, u32[]{:S(2)}, u32[]{:S(2)}) async-start(bf16[8,32,2048]{2,1,0:T(8,128)(2,1)} %bitcast.37), calls=%async_computation.1 | async-start | bytes 2097152 | tf_op jit(solution)/shard_map/all_to_all | solution.py:97
Sparse Core Ops, SparseCore 0:
  12.5 49.0 all-gather.5
where the time goes:
time: 127 us
  waiting for transfers between devices  24 us (19%)
  matrix products  21.1 us (17%)
  blocking collectives  19.9 us (16%)
  local copies, waits for them, and re-layouts  16.8 us (13%)
  starting transfers between devices  15.4 us (12%)
  between operations  14.5 us (11%)
  other arithmetic  8.99 us (7%)
  loops' own time  6.13 us (5%)
    all_gather x2, blocking collectives, collected_together(): both, at, found = (lax.all_gather(jnp.concatenate(lines), axis), 0, {})  19.9 us
    all_to_all x1, waiting for transfers between devices, sum_at_owner(): lax.all_to_all(parts, axis, split_axis=0, concat_axis=0, tiled=True)  14.4 us
    all_gather x1, waiting for transfers between devices, sent_together(): lax.all_gather(both, axis, axis=dim, tiled=True)  9.63 us
    all_to_all x1, starting transfers between devices, from_everyone(): lax.all_to_all(jnp.broadcast_to(shard[None], (count, *shard.shape)), axis...  8.59 us
    dynamic_slice x8, local copies, waits for them, and re-layouts, fold_advance(): value_block = lax.dynamic_slice_in_dim(value_rows, begin, width, 0)  7.95 us
    all_to_all x1, starting transfers between devices, sum_at_owner(): lax.all_to_all(parts, axis, split_axis=0, concat_axis=0, tiled=True)  6.73 us
    another operation x1, loops' own time, attend(): lax.scan(fold_advance, carried, jnp.arange(length // width, dtype=jnp.int...  5.92 us
    dynamic_slice x8, local copies, waits for them, and re-layouts, attend(): lax.scan(fold_advance, carried, jnp.arange(length // width, dtype=jnp.int...  4.69 us
  transfers between devices with their start and end apart: 3, of which 2 were waited for; matrix products, arithmetic and copies ran while one was open for 11% of the time, Pallas kernels for 0%

commit v1 on v0

v1 whole, which is shorter than its diff:
```python
import jax
import jax.numpy as jnp
from jax import lax
from jax.experimental import pallas as pl
from jax.experimental.pallas import tpu as pltpu
from jax.sharding import PartitionSpec as P

F32 = jnp.float32
BF16 = jnp.bfloat16
MESH = pl.DeviceIdType.MESH
EPSILON = 1e-06
ROWS = 256
WIDTH = 2048
LANES = 128
HALF = 64
SHARDS = 16
RING = 4
CHUNKS = 4
CHUNK = WIDTH // CHUNKS
STATE_MSG = 144
KV_SENDS = 80
NEGATIVE = -1e30


def dot(a, b):
    return jnp.dot(a, b, preferred_element_type=F32)


def dot_nt(a, b):
    return lax.dot_general(a, b, (((1,), (1,)), ((), ())), preferred_element_type=F32)


def split2(v):
    hi = v.astype(BF16)
    return hi, (v - hi.astype(F32)).astype(BF16)


def split3(v):
    hi = v.astype(BF16)
    rest = v - hi.astype(F32)
    mid = rest.astype(BF16)
    return hi, mid, (rest - mid.astype(F32)).astype(BF16)


def iota(shape, dim):
    return lax.broadcasted_iota(jnp.int32, shape, dim)


def kernel(
    x_hbm, xg_hbm, wq_hbm, wk_hbm, wv_hbm, qg_hbm, kg_hbm, gate_hbm, ag_hbm,
    wrq_hbm, wf_hbm, wrv_hbm, wog_hbm, slack_hbm, extra_hbm, rg_hbm, woa_hbm, wor_hbm,
    mixed_ref, lse_ref,
    x_v, n_v, xg_v, qg_v, kg_v, ag_v, slack_v, extra_v, rg_v,
    wkv, wfr, wqq, wog, wo_own, wo_peer,
    gates, kv, q_v, m_v, acc_v,
    st_row, st_col, in_v, rec_v, visq_v, outgate_v,
    act, act_peer, part, xt, xd, xs, xsum,
    lsem, gsem, grecv, ssem, krecv, rsem, rrecv, csem, crecv, psem, precv, xsem, xrecv,
):
    sp = lax.axis_index("sp")
    tp = lax.axis_index("tp")
    z, y = sp // RING, sp % RING
    xc, core = tp // 2, tp % 2
    peer = 2 * xc + 1 - core

    loads = {}

    def load(name, src, dst):
        cp = pltpu.make_async_copy(src, dst, lsem.at[len(loads)])
        cp.start()
        loads[name] = cp

    load("x", x_hbm, x_v)
    load("xg", xg_hbm, xg_v)
    load("wk", wk_hbm, wkv.at[:, pl.ds(0, LANES)])
    load("wv", wv_hbm, wkv.at[:, pl.ds(LANES, LANES)])
    load("kg", kg_hbm, kg_v)
    load("gate", gate_hbm, gates.at[sp])
    load("wf", wf_hbm, wfr.at[:, pl.ds(0, LANES)])
    load("wrv", wrv_hbm, wfr.at[:, pl.ds(LANES, LANES)])
    load("slack", slack_hbm, slack_v)
    load("extra", extra_hbm, extra_v)
    load("wq", wq_hbm, wqq.at[:, pl.ds(0, LANES)])
    load("wrq", wrq_hbm, wqq.at[:, pl.ds(LANES, LANES)])
    load("qg", qg_hbm, qg_v)
    load("wog", wog_hbm, wog)
    load("ag", ag_hbm, ag_v)
    load("rg", rg_hbm, rg_v)
    load("woa", woa_hbm, wo_own.at[pl.ds(0, LANES)])
    load("wor", wor_hbm, wo_own.at[pl.ds(LANES, LANES)])

    barrier = pltpu.get_barrier_semaphore()
    for k in range(1, SHARDS):
        pl.semaphore_signal(barrier, inc=1, device_id=((sp + k) % SHARDS, tp), device_id_type=MESH)
    x_right = 2 * ((xc + 1) % RING) + core
    x_left = 2 * ((xc + 3) % RING) + core
    for other in (x_right, x_left, peer):
        pl.semaphore_signal(barrier, inc=1, device_id=(sp, other), device_id_type=MESH)

    pending = []

    def start(pred, cp):
        if pred is None:
            cp.start()
        else:
            pl.when(pred)(cp.start)
        pending.append((pred, cp))

    loads["x"].wait()
    loads["xg"].wait()
    step = 32
    for r in range(0, ROWS, step):
        xf = x_v[r : r + step, :].astype(F32)
        mean = jnp.sum(xf * xf, axis=-1, keepdims=True) * (1.0 / WIDTH)
        n_v[r : r + step, :] = (xf * lax.rsqrt(mean + EPSILON) * xg_v[...]).astype(BF16)

    lane = iota((ROWS, LANES), 1)
    low = lane < HALF
    same_half = (iota((LANES, LANES), 0) // HALF == iota((LANES, LANES), 1) // HALF)
    halves = jnp.where(same_half, 1.0, 0.0).astype(BF16)

    def half_rms(v, gain):
        hi, lo = split2(v * v)
        mean = (dot(hi, halves) + dot(lo, halves)) * (1.0 / HALF)
        return v * lax.rsqrt(mean + EPSILON) * gain

    loads["wk"].wait()
    loads["wv"].wait()
    loads["kg"].wait()
    kv_f = dot(n_v[...], wkv[...])
    keys = half_rms(kv_f[:, :LANES], kg_v[...])
    swapped = pltpu.roll(kv_f[:, LANES:], HALF, 1)
    kv[0, sp] = jnp.where(low, keys, swapped).astype(BF16)
    kv[1, sp] = jnp.where(low, swapped, keys).astype(BF16)

    loads["gate"].wait()
    pl.semaphore_wait(barrier, SHARDS - 1 + 3)

    y_up = z * RING + (y + 1) % RING
    y_down = z * RING + (y + 3) % RING
    count = [0]

    def send(pred, h, j, target):
        n = count[0]
        count[0] += 1
        start(
            pred,
            pltpu.make_async_remote_copy(
                src_ref=kv.at[h, j], dst_ref=kv.at[h, j], send_sem=ssem.at[n], recv_sem=krecv.at[h, j],
                device_id=(target, tp), device_id_type=MESH,
            ),
        )

    def arrive(pred, h, j):
        cp = pltpu.make_async_remote_copy(
            src_ref=kv.at[h, j], dst_ref=kv.at[h, j], send_sem=ssem.at[0], recv_sem=krecv.at[h, j],
            device_id=(sp, peer), device_id_type=MESH,
        )
        if pred is None:
            cp.wait_recv()
        else:
            pl.when(pred)(cp.wait_recv)

    def send_along_z(h, j):
        send(z < 3, h, j, (sp + RING) % SHARDS)
        send(z == 0, h, j, 3 * RING + y)
        send((z == 1) & (core == 1), h, j, y)

    def send_along_y(pred, h, j):
        send(pred, h, j, y_up)
        send(pred, h, j, y_down)

    send_along_y(None, 0, sp)
    send_along_z(1, sp)
    send_along_y(None, 1, sp)
    send_along_z(0, sp)

    def gate_copy(j, target):
        return pltpu.make_async_remote_copy(
            src_ref=gates.at[j], dst_ref=gates.at[j], send_sem=gsem.at[target], recv_sem=grecv.at[j],
            device_id=(target, tp), device_id_type=MESH,
        )

    for k in range(1, SHARDS):
        target = (sp + k) % SHARDS
        start(sp + k < SHARDS, gate_copy(sp, target))

    loads["wf"].wait()
    loads["wrv"].wait()
    loads["slack"].wait()
    loads["extra"].wait()
    fr = dot(n_v[...], wfr[...])
    forget = slack_v[...] * (1.0 / (1.0 + jnp.exp(fr[:, :LANES])))
    rec_value = fr[:, LANES:].astype(BF16)
    extra = jnp.broadcast_to(extra_v[...], (LANES, ROWS)).T
    row_at, col_at = iota((ROWS, ROWS), 0), iota((ROWS, ROWS), 1)
    causal = col_at <= row_at
    lower = jnp.where(causal, 1.0, 0.0).astype(BF16)
    sums = dot(lower, jnp.concatenate(split3(jnp.log1p(-forget)) + split3(extra), axis=1))
    share_sum = sums[:, :LANES] + sums[:, LANES : 2 * LANES] + sums[:, 2 * LANES : 3 * LANES]
    extra_sum = sums[:, 3 * LANES : 4 * LANES] + sums[:, 4 * LANES : 5 * LANES] + sums[:, 5 * LANES :]
    share_end = share_sum[ROWS - 1 :, :]
    extra_end = extra_sum[ROWS - 1 :, :]
    closing = (forget * jnp.exp((share_end - share_sum) + (extra_end - extra_sum))).astype(BF16)
    state_t = dot(fr[:, LANES:].T.astype(BF16), closing)

    def state_message(state, decay):
        hi, mid, lo = (part.astype(F32) for part in split3(decay))
        at = iota((16, LANES), 0)
        tail = jnp.where(at == 0, hi, jnp.where(at == 1, mid, jnp.where(at == 2, lo, 0.0)))
        return state.astype(BF16), tail.astype(BF16)

    body, tail = state_message(state_t, share_end + extra_end)
    st_row[y, :LANES] = body
    st_row[y, LANES:] = tail

    def row_copy(j, target, n):
        return pltpu.make_async_remote_copy(
            src_ref=st_row.at[j], dst_ref=st_row.at[j], send_sem=rsem.at[n], recv_sem=rrecv.at[j],
            device_id=(target, tp), device_id_type=MESH,
        )

    def col_copy(j, target, n):
        return pltpu.make_async_remote_copy(
            src_ref=st_col.at[j], dst_ref=st_col.at[j], send_sem=csem.at[n], recv_sem=crecv.at[j],
            device_id=(target, tp), device_id_type=MESH,
        )

    for n in range(1, RING):
        start(None, row_copy(y, z * RING + (y + n) % RING, n))

    loads["wq"].wait()
    loads["wrq"].wait()
    loads["qg"].wait()
    qq = dot(n_v[...], wqq[...])
    queries = (half_rms(qq[:, :LANES], qg_v[...]).astype(BF16).astype(F32)) * (HALF**-0.5)
    q_v[0] = jnp.where(low, queries, 0.0).astype(BF16)
    q_v[1] = jnp.where(low, 0.0, queries).astype(BF16)

    rq = qq[:, LANES:]
    rec_query = rq / (1.0 + jnp.exp(-rq))
    scores = dot_nt((rec_query * jnp.exp(share_sum)).astype(BF16), (forget * jnp.exp(-share_sum)).astype(BF16))
    differ = jnp.concatenate([extra_sum, extra_sum], axis=1) - extra_sum.T[:1, :]
    scores = scores * jnp.exp(jnp.where(causal, differ, NEGATIVE))
    rec_v[...] = dot(scores.astype(BF16), rec_value)
    visq_v[...] = (rec_query * jnp.exp(share_sum + extra_sum)).astype(BF16)

    loads["wog"].wait()
    og = dot(n_v[...], wog[...])
    outgate_v[...] = og / (1.0 + jnp.exp(-og))

    def attend(j, first):
        for h in range(2):
            block = kv[h, j]
            s = dot_nt(q_v[h], block) - gates[j, h : h + 1, :]
            if first:
                s = jnp.where(causal, s, NEGATIVE)
            top = jnp.max(s, axis=-1, keepdims=True)
            if not first:
                old = m_v[h]
                top = jnp.maximum(old[:, :1], top)
            weights = jnp.exp(s - top).astype(BF16)
            ones = jnp.ones_like(block)
            right = jnp.where(low, ones, block) if h == 0 else jnp.where(low, block, ones)
            summed = dot(weights, right)
            if not first:
                summed = summed + acc_v[h] * jnp.exp(old - top)
            acc_v[h] = summed
            m_v[h] = jnp.broadcast_to(top, (ROWS, LANES))

    attend(sp, True)

    loads["woa"].wait()
    loads["wor"].wait()
    wo_copy = pltpu.make_async_remote_copy(
        src_ref=wo_own, dst_ref=wo_peer, send_sem=psem.at[0], recv_sem=precv.at[0],
        device_id=(sp, peer), device_id_type=MESH,
    )
    start(None, wo_copy)

    def wait_gates():
        for k in range(1, SHARDS):
            j = (sp + SHARDS - k) % SHARDS
            pl.when(sp >= k)(gate_copy(j, j).wait_recv)

    wait_gates()

    hops = {0: 0, 1: 1, 3: 1, 2: 2}
    plan = sorted(
        ((back, up) for back in (0, 1, 3, 2) for up in (0, 1, 3, 2) if (back, up) != (0, 0)),
        key=lambda e: hops[e[0]] + hops[e[1]],
    )

    def shard_of(back, up):
        return ((z + RING - back) % RING) * RING + (y + up) % RING

    def relay_z(valid, h, j, back):
        if back == 1:
            send((z == 1) & (core == 0) | (z == 2) & (core == 0), h, j, (sp + RING) % SHARDS)
        if back == 3:
            send((z == 3) & (core == 1), h, j, 2 * RING + y)

    def handle(h, back, up):
        valid = None if back == 0 else z >= back
        j = shard_of(back, up)
        arrive(valid, h, j)
        if h == 0:
            if back == 0:
                if up == 3:
                    send(core == 0, h, j, y_up)
                if up == 1:
                    send(core == 1, h, j, y_down)
                send_along_z(h, j)
            else:
                relay_z(valid, h, j, back)
        else:
            if up == 0:
                relay_z(valid, h, j, back)
                send_along_y(valid, h, j)
            else:
                fine = core == (0 if up == 3 else 1)
                if up != 2:
                    send(fine if valid is None else fine & valid, h, j, y_up if up == 3 else y_down)
        if back == 1 and (h == 0 or up == 0):
            through = (z == 0) & (core == 1)
            jj = RING + (y + up) % RING
            arrive(through, h, jj)
            send(through, h, jj, 3 * RING + y)

    def compute(back, up):
        needed = (z >= back) if back else (y + up) % RING < y
        j = shard_of(back, up)

        @pl.when(needed)
        def _():
            attend(j, False)

    def read_state(ref, j):
        tail = ref[j, LANES:].astype(F32)
        return ref[j, :LANES].astype(F32), tail[0:1] + tail[1:2] + tail[2:3]

    def combine_row():
        for n in range(1, RING):
            row_copy((y + n) % RING, sp, n).wait_recv()
        before, decay = jnp.zeros((LANES, LANES), F32), jnp.zeros((1, LANES), F32)
        mine, mine_decay = before, decay
        for k in range(RING):
            state, log = read_state(st_row, k)
            before = jnp.exp(log) * before + state
            decay = decay + log
            mine = jnp.where(k < y, before, mine)
            mine_decay = jnp.where(k < y, decay, mine_decay)
        in_v[0] = mine
        in_v[1, 0:1] = mine_decay
        body, tail = state_message(before, decay)
        st_col[z, :LANES] = body
        st_col[z, LANES:] = tail
        for n in range(1, RING):
            start(z + n < RING, col_copy(z, ((z + n) % RING) * RING + y, n))

    def combine_col():
        for n in range(1, RING):
            pl.when(z >= n)(col_copy((z + RING - n) % RING, sp, n).wait_recv)
        in_v[2] = jnp.zeros((LANES, LANES), F32)
        for k in range(RING - 1):

            @pl.when(k < z)
            def _():
                state, log = read_state(st_col, k)
                in_v[2] = jnp.exp(log) * in_v[2] + state

        incoming = jnp.exp(in_v[1, 0:1]) * in_v[2] + in_v[0]
        recurrent = rec_v[...] + dot_nt(visq_v[...], incoming.astype(BF16))
        mean = jnp.mean(recurrent * recurrent, axis=-1, keepdims=True)
        return (recurrent * lax.rsqrt(mean + EPSILON) * rg_v[...] * outgate_v[...]).astype(BF16)

    last = None
    for i, (back, up) in enumerate(plan):
        handle(0, back, up)
        handle(1, back, up)
        if last is not None:
            compute(*last)
        last = (back, up)
        if i == 5:
            combine_row()
    loads["ag"].wait()
    loads["rg"].wait()
    rec_out = combine_col()
    compute(*last)

    a0, a1 = acc_v[0], acc_v[1]
    totals = jnp.where(low, a0, a1)
    attention = pltpu.roll(jnp.where(low, a1, a0), HALF, 1) / totals
    attn_out = half_rms(attention, ag_v[...]).astype(BF16)
    for b in range(8):
        rows = slice(32 * b, 32 * b + 32)
        at = slice(32 * (b // 2), 32 * (b // 2) + 32)
        act[b % 2, at, :LANES] = attn_out[rows]
        act[b % 2, at, LANES:] = rec_out[rows]
    act_copy = pltpu.make_async_remote_copy(
        src_ref=act.at[1 - core], dst_ref=act_peer, send_sem=psem.at[1], recv_sem=precv.at[1],
        device_id=(sp, peer), device_id_type=MESH,
    )
    start(None, act_copy)
    log_sum = (jnp.where(low, m_v[0], m_v[1]) + jnp.log(totals)).T
    lse_ref[0:1, :] = log_sum[0:1, :] + gates[sp, 0:1, :]
    lse_ref[1:2, :] = log_sum[HALF : HALF + 1, :] + gates[sp, 1:2, :]
    wo_copy.wait_recv()
    act_copy.wait_recv()

    e_next = (xc + 2 * core + 3) % RING
    e_prev = (xc + 5 - 2 * core) % RING
    far = (xc + 2) % RING
    to_next = 2 * e_next + core
    to_prev = 2 * e_prev + core

    def x_copy(kind, c, src, dst, target):
        return pltpu.make_async_remote_copy(
            src_ref=src, dst_ref=dst, send_sem=xsem.at[kind, c], recv_sem=xrecv.at[kind, c],
            device_id=(sp, target), device_id_type=MESH,
        )

    mine = act[core]
    theirs = act_peer[...]
    for c in range(CHUNKS):
        cols = slice(c * CHUNK, (c + 1) * CHUNK)
        product = dot(mine, wo_own[:, cols]) + dot(theirs, wo_peer[:, cols])
        for b in range(RING):
            part[c, b] = product[32 * b : 32 * b + 32].astype(BF16)
        start(None, x_copy(0, c, part.at[c, far], xt.at[c], to_next))
        start(None, x_copy(1, c, part.at[c, e_prev], xd.at[c], to_prev))
    for c in range(CHUNKS):
        x_copy(0, c, part.at[c, far], xt.at[c], to_next).wait_recv()
        xsum[c] = (xt[c].astype(F32) + part[c, e_next].astype(F32)).astype(BF16)
        start(None, x_copy(2, c, xsum.at[c], xs.at[c], to_next))
    for c in range(CHUNKS):
        x_copy(1, c, part.at[c, e_prev], xd.at[c], to_prev).wait_recv()
        x_copy(2, c, xsum.at[c], xs.at[c], to_next).wait_recv()
        total = part[c, xc].astype(F32) + xd[c].astype(F32) + xs[c].astype(F32)
        mixed_ref[:, c * CHUNK : (c + 1) * CHUNK] = total.astype(BF16)
    for pred, cp in pending:
        if pred is None:
            cp.wait_send()
        else:
            pl.when(pred)(cp.wait_send)


def body(*args):
    (
        layer_input_rows, input_norm_gain, query_weight, key_weight, value_weight, query_norm_gain,
        key_norm_gain, cumulative_gate, attention_norm_gain, recurrence_query_weight, forget_weight,
        recurrence_value_weight, output_gate_weight, gate_lower_slack, extra_log_decay,
        recurrence_norm_gain, attention_output_weight, recurrence_output_weight,
    ) = args
    twice = lambda gain: jnp.concatenate([gain, gain])[None]
    operands = (
        layer_input_rows, input_norm_gain[None], query_weight, key_weight, value_weight,
        twice(query_norm_gain), twice(key_norm_gain), cumulative_gate.T, attention_norm_gain[None],
        recurrence_query_weight, forget_weight, recurrence_value_weight, output_gate_weight,
        gate_lower_slack[None], extra_log_decay.T, recurrence_norm_gain[None],
        attention_output_weight, recurrence_output_weight,
    )
    dma = pltpu.SemaphoreType.DMA
    mixed, lse = pl.pallas_call(
        kernel,
        name="mixer",
        out_shape=(
            jax.ShapeDtypeStruct((ROWS // 8, WIDTH), BF16),
            jax.ShapeDtypeStruct((2, ROWS), F32),
        ),
        in_specs=[pl.BlockSpec(memory_space=pl.ANY)] * len(operands),
        out_specs=(pl.BlockSpec(memory_space=pltpu.VMEM), pl.BlockSpec(memory_space=pltpu.VMEM)),
        scratch_shapes=[
            pltpu.VMEM((ROWS, WIDTH), BF16),
            pltpu.VMEM((ROWS, WIDTH), BF16),
            pltpu.VMEM((1, WIDTH), F32),
            pltpu.VMEM((1, LANES), F32),
            pltpu.VMEM((1, LANES), F32),
            pltpu.VMEM((1, LANES), F32),
            pltpu.VMEM((1, LANES), F32),
            pltpu.VMEM((1, ROWS), F32),
            pltpu.VMEM((1, LANES), F32),
            pltpu.VMEM((WIDTH, 2 * LANES), BF16),
            pltpu.VMEM((WIDTH, 2 * LANES), BF16),
            pltpu.VMEM((WIDTH, 2 * LANES), BF16),
            pltpu.VMEM((WIDTH, LANES), BF16),
            pltpu.VMEM((2 * LANES, WIDTH), BF16),
            pltpu.VMEM((2 * LANES, WIDTH), BF16),
            pltpu.VMEM((SHARDS, 2, ROWS), F32),
            pltpu.VMEM((2, SHARDS, ROWS, LANES), BF16),
            pltpu.VMEM((2, ROWS, LANES), BF16),
            pltpu.VMEM((2, ROWS, LANES), F32),
            pltpu.VMEM((2, ROWS, LANES), F32),
            pltpu.VMEM((RING, STATE_MSG, LANES), BF16),
            pltpu.VMEM((RING, STATE_MSG, LANES), BF16),
            pltpu.VMEM((3, LANES, LANES), F32),
            pltpu.VMEM((ROWS, LANES), F32),
            pltpu.VMEM((ROWS, LANES), BF16),
            pltpu.VMEM((ROWS, LANES), F32),
            pltpu.VMEM((2, ROWS // 2, 2 * LANES), BF16),
            pltpu.VMEM((ROWS // 2, 2 * LANES), BF16),
            pltpu.VMEM((CHUNKS, RING, ROWS // 8, CHUNK), BF16),
            pltpu.VMEM((CHUNKS, ROWS // 8, CHUNK), BF16),
            pltpu.VMEM((CHUNKS, ROWS // 8, CHUNK), BF16),
            pltpu.VMEM((CHUNKS, ROWS // 8, CHUNK), BF16),
            pltpu.VMEM((CHUNKS, ROWS // 8, CHUNK), BF16),
            dma((18,)),
            dma((SHARDS,)),
            dma((SHARDS,)),
            dma((KV_SENDS,)),
            dma((2, SHARDS)),
            dma((RING,)),
            dma((RING,)),
            dma((RING,)),
            dma((RING,)),
            dma((2,)),
            dma((2,)),
            dma((3, CHUNKS)),
            dma((3, CHUNKS)),
        ],
        compiler_params=pltpu.CompilerParams(
            collective_id=0, has_side_effects=True, vmem_limit_bytes=60 * 1024 * 1024
        ),
    )(*operands)
    return mixed, lse.T


def solution(mesh):
    both = P("sp", "tp")
    placed = (
        P("sp", None), P(), P(None, "tp"), P(None, "tp"), P(None, "tp"), P(), P(), both, P("tp"),
        P(None, "tp"), P(None, "tp"), P(None, "tp"), P(None, "tp"), P("tp"), both, P("tp"),
        P("tp", None), P("tp", None),
    )
    return jax.shard_map(
        body, mesh=mesh, in_specs=placed, out_specs=(P(("sp", "tp"), None), both), check_vma=False
    )
```

time: 127 us -> 48.3 us (0.38)
  the two profiles are of different devices: /device:TPU:1 before, /device:TPU:97 now
where the time goes in v1:
time: 48.3 us; the launch traced here: 48.2 us
  Pallas kernels  44.1 us (91%)
  local copies, waits for them, and re-layouts  2.81 us (6%)
  between operations  0.66 us (1%)
  other arithmetic  0.59 us (1%)
    pallas_call x1, Pallas kernels, body(): pl.pallas_call(kernel, name='mixer', out_shape=(jax.ShapeDtypeStruct((ROW...  44.1 us
    unnamed x8, local copies, waits for them, and re-layouts  2.81 us

profile of v1, /device:TPU:97, one launch (start us, length us, event | category | flops | bytes accessed | tf_op | source)
XLA Modules:
  0.0 48.2 jit_solution(6456165581989510140)
XLA Ops:
  0.6 0.0 copy-start.1
  0.6 0.0 copy-start.2
  0.6 0.6 %copy-done.1 = f32[64]{0:T(128)S(1)} copy-done((f32[64]{0:T(128)S(1)}, f32[64]{0:T(128)}, u32[]{:S(2)}) %copy-start.1) | copy-done | bytes 280
  1.3 0.0 copy-done.2
  1.3 0.6 %maximum_bitcast_fusion = (f32[1,128]{1,0:T(1,128)}, f32[1,128]{1,0:T(1,128)}) fusion(f32[64]{0:T(128)S(1)} %copy-done.1, f32[64]{0:T(128)S(1)} %copy-done.2), kind=kLoop, calls=%fused_computation | loop fusion | flops 256 | bytes 1536 | tf_op jit(solution)/shard_map/broadcast_in_dim | solution.py:455
  1.9 44.1 %mixer.1 = (bf16[32,2048]{1,0:T(8,128)(2,1)}, f32[2,256]{1,0:T(2,128)}) custom-call(bf16[256,2048]{1,0:T(8,128)(2,1)} %x_hbm.1, f32[1,2048]{1,0:T(1,128)} %bitcast.11, bf16[2048,128]{1,0:T(8,128)(2,1)} %wq_hbm.1, bf16[2048,128]{1,0:T(8,128)(2,1)} %wk_hbm.1, bf16[2048,128]{1,0:T(8,128)(2,1)} %wv_hbm.1, f32[1,128]{1,0:T(1,128)} %get-tuple-element.6.qg_hbm, ...), custom_call_target="tpu_custom_call" | custom-call | tf_op jit(solution)/shard_map/mixer/pallas_call | solution.py:464
  46.0 0.0 copy-start
  46.0 1.6 %copy.22 = bf16[32,2048]{1,0:T(8,128)(2,1)} copy(bf16[32,2048]{1,0:T(8,128)(2,1)} %get-tuple-element.10) | data formatting | bytes 262144
  47.6 0.0 copy-done
  47.6 0.6 %copy.23 = f32[256,2]{0,1:T(2,128)} copy(f32[256,2]{0,1:T(2,128)S(1)} %bitcast.13) | data formatting | bytes 4096
Async XLA Ops:
  0.6 0.7 %copy-start.1 = (f32[64]{0:T(128)S(1)}, f32[64]{0:T(128)}, u32[]{:S(2)}) copy-start(f32[64]{0:T(128)} %param.23) | copy-start | bytes 772
  0.6 0.7 %copy-start.2 = (f32[64]{0:T(128)S(1)}, f32[64]{0:T(128)}, u32[]{:S(2)}) copy-start(f32[64]{0:T(128)} %param.24) | copy-start | bytes 772
  46.0 1.6 %copy-start = (f32[2,256]{1,0:T(2,128)S(1)}, f32[2,256]{1,0:T(2,128)}, u32[]{:S(2)}) copy-start(f32[2,256]{1,0:T(2,128)} %get-tuple-element.5) | copy-start | bytes 6148

commit v2 on v1

--- a/solution.py
+++ b/solution.py
@@ -119,6 +119,9 @@
     same_half = (iota((LANES, LANES), 0) // HALF == iota((LANES, LANES), 1) // HALF)
     halves = jnp.where(same_half, 1.0, 0.0).astype(BF16)
 
+    def twice(gain):
+        return jnp.concatenate([gain, gain], axis=1)
+
     def half_rms(v, gain):
         hi, lo = split2(v * v)
         mean = (dot(hi, halves) + dot(lo, halves)) * (1.0 / HALF)
@@ -128,7 +131,7 @@
     loads["wv"].wait()
     loads["kg"].wait()
     kv_f = dot(n_v[...], wkv[...])
-    keys = half_rms(kv_f[:, :LANES], kg_v[...])
+    keys = half_rms(kv_f[:, :LANES], twice(kg_v[...]))
     swapped = pltpu.roll(kv_f[:, LANES:], HALF, 1)
     kv[0, sp] = jnp.where(low, keys, swapped).astype(BF16)
     kv[1, sp] = jnp.where(low, swapped, keys).astype(BF16)
@@ -170,11 +173,6 @@
         send(pred, h, j, y_up)
         send(pred, h, j, y_down)
 
-    send_along_y(None, 0, sp)
-    send_along_z(1, sp)
-    send_along_y(None, 1, sp)
-    send_along_z(0, sp)
-
     def gate_copy(j, target):
         return pltpu.make_async_remote_copy(
             src_ref=gates.at[j], dst_ref=gates.at[j], send_sem=gsem.at[target], recv_sem=grecv.at[j],
@@ -184,6 +182,11 @@
     for k in range(1, SHARDS):
         target = (sp + k) % SHARDS
         start(sp + k < SHARDS, gate_copy(sp, target))
+
+    send_along_y(None, 0, sp)
+    send_along_z(1, sp)
+    send_along_y(None, 1, sp)
+    send_along_z(0, sp)
 
     loads["wf"].wait()
     loads["wrv"].wait()
@@ -233,7 +236,7 @@
     loads["wrq"].wait()
     loads["qg"].wait()
     qq = dot(n_v[...], wqq[...])
-    queries = (half_rms(qq[:, :LANES], qg_v[...]).astype(BF16).astype(F32)) * (HALF**-0.5)
+    queries = (half_rms(qq[:, :LANES], twice(qg_v[...])).astype(BF16).astype(F32)) * (HALF**-0.5)
     q_v[0] = jnp.where(low, queries, 0.0).astype(BF16)
     q_v[1] = jnp.where(low, 0.0, queries).astype(BF16)
 
@@ -249,26 +252,34 @@
     og = dot(n_v[...], wog[...])
     outgate_v[...] = og / (1.0 + jnp.exp(-og))
 
-    def attend(j, first):
+    def attend(blocks, first=False, shown=None):
         for h in range(2):
-            block = kv[h, j]
-            s = dot_nt(q_v[h], block) - gates[j, h : h + 1, :]
-            if first:
-                s = jnp.where(causal, s, NEGATIVE)
-            top = jnp.max(s, axis=-1, keepdims=True)
+            parts = []
+            for i, j in enumerate(blocks):
+                gate = gates[j, h : h + 1, :]
+                if shown is not None:
+                    gate = jnp.where(shown[i], gate, -NEGATIVE)
+                part = dot_nt(q_v[h], kv[h, j]) - gate
+                parts.append(jnp.where(causal, part, NEGATIVE) if first else part)
+            widest = parts[0]
+            for part in parts[1:]:
+                widest = jnp.maximum(widest, part)
+            top = jnp.max(widest, axis=-1, keepdims=True)
             if not first:
                 old = m_v[h]
                 top = jnp.maximum(old[:, :1], top)
-            weights = jnp.exp(s - top).astype(BF16)
-            ones = jnp.ones_like(block)
-            right = jnp.where(low, ones, block) if h == 0 else jnp.where(low, block, ones)
-            summed = dot(weights, right)
-            if not first:
-                summed = summed + acc_v[h] * jnp.exp(old - top)
+            summed = None if first else acc_v[h] * jnp.exp(old - top)
+            for part, j in zip(parts, blocks):
+                weights = jnp.exp(part - top).astype(BF16)
+                block = kv[h, j]
+                ones = jnp.ones_like(block)
+                right = jnp.where(low, ones, block) if h == 0 else jnp.where(low, block, ones)
+                term = dot(weights, right)
+                summed = term if summed is None else summed + term
             acc_v[h] = summed
             m_v[h] = jnp.broadcast_to(top, (ROWS, LANES))
 
-    attend(sp, True)
+    attend([sp], first=True)
 
     loads["woa"].wait()
     loads["wor"].wait()
@@ -278,12 +289,8 @@
     )
     start(None, wo_copy)
 
-    def wait_gates():
-        for k in range(1, SHARDS):
-            j = (sp + SHARDS - k) % SHARDS
-            pl.when(sp >= k)(gate_copy(j, j).wait_recv)
-
-    wait_gates()
+    def wait_gate(valid, j):
+        pl.when(valid)(gate_copy(j, j).wait_recv)
 
     hops = {0: 0, 1: 1, 3: 1, 2: 2}
     plan = sorted(
@@ -327,13 +334,23 @@
             arrive(through, h, jj)
             send(through, h, jj, 3 * RING + y)
 
-    def compute(back, up):
-        needed = (z >= back) if back else (y + up) % RING < y
-        j = shard_of(back, up)
-
-        @pl.when(needed)
+    def attend_own_row():
+        blocks = [shard_of(0, up) for up in (1, 2, 3)]
+        shown = [y + up >= RING for up in (1, 2, 3)]
+        for valid, j in zip(shown, blocks):
+            wait_gate(valid, j)
+
+        @pl.when(y > 0)
         def _():
-            attend(j, False)
+            attend(blocks, shown=shown)
+
+    def attend_row(back, ups):
+        @pl.when(z >= back)
+        def _():
+            blocks = [shard_of(back, up) for up in ups]
+            for j in blocks:
+                gate_copy(j, j).wait_recv()
+            attend(blocks)
 
     def read_state(ref, j):
         tail = ref[j, LANES:].astype(F32)
@@ -374,19 +391,25 @@
         mean = jnp.mean(recurrent * recurrent, axis=-1, keepdims=True)
         return (recurrent * lax.rsqrt(mean + EPSILON) * rg_v[...] * outgate_v[...]).astype(BF16)
 
-    last = None
-    for i, (back, up) in enumerate(plan):
-        handle(0, back, up)
-        handle(1, back, up)
-        if last is not None:
-            compute(*last)
-        last = (back, up)
-        if i == 5:
-            combine_row()
+    def handle_level(level):
+        for back, up in plan:
+            if hops[back] + hops[up] == level:
+                handle(0, back, up)
+                handle(1, back, up)
+
+    handle_level(1)
+    handle_level(2)
+    combine_row()
+    attend_own_row()
+    handle_level(3)
+    attend_row(1, (0, 1, 3, 2))
+    attend_row(3, (0, 1, 3, 2))
+    attend_row(2, (0, 1, 3))
     loads["ag"].wait()
     loads["rg"].wait()
     rec_out = combine_col()
-    compute(*last)
+    handle_level(4)
+    attend_row(2, (2,))
 
     a0, a1 = acc_v[0], acc_v[1]
     totals = jnp.where(low, a0, a1)
@@ -428,6 +451,7 @@
         for b in range(RING):
             part[c, b] = product[32 * b : 32 * b + 32].astype(BF16)
         start(None, x_copy(0, c, part.at[c, far], xt.at[c], to_next))
+    for c in range(CHUNKS):
         start(None, x_copy(1, c, part.at[c, e_prev], xd.at[c], to_prev))
     for c in range(CHUNKS):
         x_copy(0, c, part.at[c, far], xt.at[c], to_next).wait_recv()
@@ -452,10 +476,9 @@
         recurrence_value_weight, output_gate_weight, gate_lower_slack, extra_log_decay,
         recurrence_norm_gain, attention_output_weight, recurrence_output_weight,
     ) = args
-    twice = lambda gain: jnp.concatenate([gain, gain])[None]
     operands = (
         layer_input_rows, input_norm_gain[None], query_weight, key_weight, value_weight,
-        twice(query_norm_gain), twice(key_norm_gain), cumulative_gate.T, attention_norm_gain[None],
+        query_norm_gain[None], key_norm_gain[None], cumulative_gate.T, attention_norm_gain[None],
         recurrence_query_weight, forget_weight, recurrence_value_weight, output_gate_weight,
         gate_lower_slack[None], extra_log_decay.T, recurrence_norm_gain[None],
         attention_output_weight, recurrence_output_weight,
@@ -468,14 +491,14 @@
             jax.ShapeDtypeStruct((ROWS // 8, WIDTH), BF16),
             jax.ShapeDtypeStruct((2, ROWS), F32),
         ),
-        in_specs=[pl.BlockSpec(memory_space=pl.ANY)] * len(operands),
+        in_specs=[pl.BlockSpec(memory_space=pltpu.HBM)] * len(operands),
         out_specs=(pl.BlockSpec(memory_space=pltpu.VMEM), pl.BlockSpec(memory_space=pltpu.VMEM)),
         scratch_shapes=[
             pltpu.VMEM((ROWS, WIDTH), BF16),
             pltpu.VMEM((ROWS, WIDTH), BF16),
             pltpu.VMEM((1, WIDTH), F32),
-            pltpu.VMEM((1, LANES), F32),
-            pltpu.VMEM((1, LANES), F32),
+            pltpu.VMEM((1, HALF), F32),
+            pltpu.VMEM((1, HALF), F32),
             pltpu.VMEM((1, LANES), F32),
             pltpu.VMEM((1, LANES), F32),
             pltpu.VMEM((1, ROWS), F32),

time: 48.3 us -> 41.1 us (0.85)
  Pallas kernels: 44.1 us -> 38.1 us
  local copies, waits for them, and re-layouts: 2.81 us -> 2.15 us
  other arithmetic: 0.59 us -> 0 us
    pallas_call x1, Pallas kernels: 44.1 us -> 38.1 us  [body(): pl.pallas_call(kernel, name='mixer', out_shape=(jax.ShapeDtypeStruct((ROW...]
    unnamed x8 -> x4, local copies, waits for them, and re-layouts: 2.81 us -> 2.15 us
    broadcast_in_dim x1 -> x0, other arithmetic: 0.59 us -> none  [body(): twice = lambda gain: jnp.concatenate([gain, gain])[None]]
where the time goes in v2:
time: 41.1 us; the launch traced here: 40.9 us
  Pallas kernels  38.1 us (93%)
  local copies, waits for them, and re-layouts  2.15 us (5%)
  between operations  0.65 us (2%)
    pallas_call x1, Pallas kernels, body(): pl.pallas_call(kernel, name='mixer', out_shape=(jax.ShapeDtypeStruct((ROW...  38.1 us
    unnamed x4, local copies, waits for them, and re-layouts  2.15 us

profile of v2, /device:TPU:97, one launch (start us, length us, event | category | flops | bytes accessed | tf_op | source)
XLA Modules:
  0.0 40.9 jit_solution(6787598779118203293)
XLA Ops:
  0.6 38.1 %mixer.1 = (bf16[32,2048]{1,0:T(8,128)(2,1)}, f32[2,256]{1,0:T(2,128)}) custom-call(bf16[256,2048]{1,0:T(8,128)(2,1)} %x_hbm.1, f32[1,2048]{1,0:T(1,128)} %bitcast.9, bf16[2048,128]{1,0:T(8,128)(2,1)} %wq_hbm.1, bf16[2048,128]{1,0:T(8,128)(2,1)} %wk_hbm.1, bf16[2048,128]{1,0:T(8,128)(2,1)} %wv_hbm.1, f32[1,64]{1,0:T(1,128)} %bitcast.13, f32[1,64]{1,0:T(1,128)} %bitcast.14, ...), custom_call_target="tpu_custom_call" | custom-call | tf_op jit(solution)/shard_map/mixer/pallas_call | solution.py:487
  38.8 0.0 copy-start
  38.8 1.6 %copy.22 = bf16[32,2048]{1,0:T(8,128)(2,1)} copy(bf16[32,2048]{1,0:T(8,128)(2,1)} %get-tuple-element.8) | data formatting | bytes 262144
  40.4 0.0 copy-done
  40.4 0.6 %copy.23 = f32[256,2]{0,1:T(2,128)} copy(f32[256,2]{0,1:T(2,128)S(1)} %bitcast.11) | data formatting | bytes 4096
Async XLA Ops:
  38.8 1.6 %copy-start = (f32[2,256]{1,0:T(2,128)S(1)}, f32[2,256]{1,0:T(2,128)}, u32[]{:S(2)}) copy-start(f32[2,256]{1,0:T(2,128)} %get-tuple-element.5) | copy-start | bytes 6148

commit v3 on v2

--- a/solution.py
+++ b/solution.py
@@ -49,12 +49,12 @@
 def kernel(
     x_hbm, xg_hbm, wq_hbm, wk_hbm, wv_hbm, qg_hbm, kg_hbm, gate_hbm, ag_hbm,
     wrq_hbm, wf_hbm, wrv_hbm, wog_hbm, slack_hbm, extra_hbm, rg_hbm, woa_hbm, wor_hbm,
-    mixed_ref, lse_ref,
+    own_ref, direct_ref, summed_ref, lse_ref,
     x_v, n_v, xg_v, qg_v, kg_v, ag_v, slack_v, extra_v, rg_v,
-    wkv, wfr, wqq, wog, wo_own, wo_peer,
+    wkv, wfr, wqq, wog, woa, wor, product_v,
     gates, kv, q_v, m_v, acc_v,
     st_row, st_col, in_v, rec_v, visq_v, outgate_v,
-    act, act_peer, part, xt, xd, xs, xsum,
+    act_r, act_a, peer_r, peer_a, part, xt, xsum,
     lsem, gsem, grecv, ssem, krecv, rsem, rrecv, csem, crecv, psem, precv, xsem, xrecv,
 ):
     sp = lax.axis_index("sp")
@@ -70,24 +70,13 @@
         cp.start()
         loads[name] = cp
 
-    load("x", x_hbm, x_v)
+    for r in range(0, ROWS, HALF):
+        load(("x", r), x_hbm.at[pl.ds(r, HALF)], x_v.at[pl.ds(r, HALF)])
     load("xg", xg_hbm, xg_v)
     load("wk", wk_hbm, wkv.at[:, pl.ds(0, LANES)])
     load("wv", wv_hbm, wkv.at[:, pl.ds(LANES, LANES)])
     load("kg", kg_hbm, kg_v)
     load("gate", gate_hbm, gates.at[sp])
-    load("wf", wf_hbm, wfr.at[:, pl.ds(0, LANES)])
-    load("wrv", wrv_hbm, wfr.at[:, pl.ds(LANES, LANES)])
-    load("slack", slack_hbm, slack_v)
-    load("extra", extra_hbm, extra_v)
-    load("wq", wq_hbm, wqq.at[:, pl.ds(0, LANES)])
-    load("wrq", wrq_hbm, wqq.at[:, pl.ds(LANES, LANES)])
-    load("qg", qg_hbm, qg_v)
-    load("wog", wog_hbm, wog)
-    load("ag", ag_hbm, ag_v)
-    load("rg", rg_hbm, rg_v)
-    load("woa", woa_hbm, wo_own.at[pl.ds(0, LANES)])
-    load("wor", wor_hbm, wo_own.at[pl.ds(LANES, LANES)])
 
     barrier = pltpu.get_barrier_semaphore()
     for k in range(1, SHARDS):
@@ -106,10 +95,24 @@
             pl.when(pred)(cp.start)
         pending.append((pred, cp))
 
-    loads["x"].wait()
     loads["xg"].wait()
     step = 32
     for r in range(0, ROWS, step):
+        if r % HALF == 0:
+            loads["x", r].wait()
+        if r == HALF:
+            load("wf", wf_hbm, wfr.at[:, pl.ds(0, LANES)])
+            load("wrv", wrv_hbm, wfr.at[:, pl.ds(LANES, LANES)])
+            load("slack", slack_hbm, slack_v)
+            load("extra", extra_hbm, extra_v)
+            load("wq", wq_hbm, wqq.at[:, pl.ds(0, LANES)])
+            load("wrq", wrq_hbm, wqq.at[:, pl.ds(LANES, LANES)])
+            load("qg", qg_hbm, qg_v)
+            load("wog", wog_hbm, wog)
+            load("ag", ag_hbm, ag_v)
+            load("rg", rg_hbm, rg_v)
+            load("woa", woa_hbm, woa.at[pl.ds(0, LANES)])
+            load("wor", wor_hbm, wor.at[pl.ds(0, LANES)])
         xf = x_v[r : r + step, :].astype(F32)
         mean = jnp.sum(xf * xf, axis=-1, keepdims=True) * (1.0 / WIDTH)
         n_v[r : r + step, :] = (xf * lax.rsqrt(mean + EPSILON) * xg_v[...]).astype(BF16)
@@ -281,13 +284,18 @@
 
     attend([sp], first=True)
 
+    def to_peer(n, src, dst):
+        return pltpu.make_async_remote_copy(
+            src_ref=src, dst_ref=dst, send_sem=psem.at[n], recv_sem=precv.at[n],
+            device_id=(sp, peer), device_id_type=MESH,
+        )
+
     loads["woa"].wait()
     loads["wor"].wait()
-    wo_copy = pltpu.make_async_remote_copy(
-        src_ref=wo_own, dst_ref=wo_peer, send_sem=psem.at[0], recv_sem=precv.at[0],
-        device_id=(sp, peer), device_id_type=MESH,
-    )
-    start(None, wo_copy)
+    wor_copy = to_peer(0, wor.at[pl.ds(0, LANES)], wor.at[pl.ds(LANES, LANES)])
+    woa_copy = to_peer(1, woa.at[pl.ds(0, LANES)], woa.at[pl.ds(LANES, LANES)])
+    start(None, wor_copy)
+    start(None, woa_copy)
 
     def wait_gate(valid, j):
         pl.when(valid)(gate_copy(j, j).wait_recv)
@@ -391,44 +399,56 @@
         mean = jnp.mean(recurrent * recurrent, axis=-1, keepdims=True)
         return (recurrent * lax.rsqrt(mean + EPSILON) * rg_v[...] * outgate_v[...]).astype(BF16)
 
-    def handle_level(level):
-        for back, up in plan:
-            if hops[back] + hops[up] == level:
-                handle(0, back, up)
-                handle(1, back, up)
-
-    handle_level(1)
-    handle_level(2)
+    def by_owner(ref, rows):
+        for b in range(8):
+            ref[b % 2, 32 * (b // 2) : 32 * (b // 2) + 32, :] = rows[32 * b : 32 * b + 32]
+
+    def share_recurrence():
+        loads["rg"].wait()
+        by_owner(act_r, combine_col())
+        start(None, to_peer(2, act_r.at[1 - core], peer_r))
+
+    def project_recurrence():
+        wor_copy.wait_recv()
+        to_peer(2, act_r.at[1 - core], peer_r).wait_recv()
+        both = jnp.concatenate([act_r[core], peer_r[...]], axis=1)
+        for c in range(CHUNKS):
+            cols = slice(c * CHUNK, (c + 1) * CHUNK)
+            product_v[:, cols] = dot(both, wor[:, cols])
+
+    def handle_all(events):
+        for h, back, up in events:
+            handle(h, back, up)
+
+    handle_all((
+        (1, 3, 0), (1, 1, 0), (0, 0, 3), (0, 0, 1), (1, 0, 1), (1, 0, 3), (0, 3, 0), (0, 3, 3), (0, 1, 0),
+        (1, 3, 1), (1, 2, 0), (1, 3, 3), (1, 1, 3), (1, 1, 1), (1, 0, 2), (0, 3, 1), (0, 0, 2), (0, 1, 1),
+    ))
+    attend_own_row()
+    handle_all(((0, 2, 0), (1, 2, 3), (0, 1, 3)))
     combine_row()
-    attend_own_row()
-    handle_level(3)
+    handle_all(((0, 3, 2), (1, 2, 1), (1, 3, 2)))
+    attend_row(3, (0, 1, 3, 2))
+    handle_all(((0, 1, 2), (1, 1, 2), (0, 2, 1)))
     attend_row(1, (0, 1, 3, 2))
-    attend_row(3, (0, 1, 3, 2))
-    attend_row(2, (0, 1, 3))
-    loads["ag"].wait()
-    loads["rg"].wait()
-    rec_out = combine_col()
-    handle_level(4)
-    attend_row(2, (2,))
+    share_recurrence()
+    handle_all(((0, 2, 3),))
+    project_recurrence()
+    handle_all(((0, 2, 2), (1, 2, 2)))
+    attend_row(2, (0, 1, 3, 2))
 
     a0, a1 = acc_v[0], acc_v[1]
     totals = jnp.where(low, a0, a1)
+    loads["ag"].wait()
     attention = pltpu.roll(jnp.where(low, a1, a0), HALF, 1) / totals
     attn_out = half_rms(attention, ag_v[...]).astype(BF16)
-    for b in range(8):
-        rows = slice(32 * b, 32 * b + 32)
-        at = slice(32 * (b // 2), 32 * (b // 2) + 32)
-        act[b % 2, at, :LANES] = attn_out[rows]
-        act[b % 2, at, LANES:] = rec_out[rows]
-    act_copy = pltpu.make_async_remote_copy(
-        src_ref=act.at[1 - core], dst_ref=act_peer, send_sem=psem.at[1], recv_sem=precv.at[1],
-        device_id=(sp, peer), device_id_type=MESH,
-    )
+    by_owner(act_a, attn_out)
+    act_copy = to_peer(3, act_a.at[1 - core], peer_a)
     start(None, act_copy)
     log_sum = (jnp.where(low, m_v[0], m_v[1]) + jnp.log(totals)).T
     lse_ref[0:1, :] = log_sum[0:1, :] + gates[sp, 0:1, :]
     lse_ref[1:2, :] = log_sum[HALF : HALF + 1, :] + gates[sp, 1:2, :]
-    wo_copy.wait_recv()
+    woa_copy.wait_recv()
     act_copy.wait_recv()
 
     e_next = (xc + 2 * core + 3) % RING
@@ -443,30 +463,41 @@
             device_id=(sp, target), device_id_type=MESH,
         )
 
-    mine = act[core]
-    theirs = act_peer[...]
+    both = jnp.concatenate([act_a[core], peer_a[...]], axis=1)
     for c in range(CHUNKS):
         cols = slice(c * CHUNK, (c + 1) * CHUNK)
-        product = dot(mine, wo_own[:, cols]) + dot(theirs, wo_peer[:, cols])
+        product = product_v[:, cols] + dot(both, woa[:, cols])
         for b in range(RING):
             part[c, b] = product[32 * b : 32 * b + 32].astype(BF16)
         start(None, x_copy(0, c, part.at[c, far], xt.at[c], to_next))
     for c in range(CHUNKS):
-        start(None, x_copy(1, c, part.at[c, e_prev], xd.at[c], to_prev))
+        start(None, x_copy(1, c, part.at[c, e_prev], direct_ref.at[c], to_prev))
+    own_copies = [
+        pltpu.make_async_copy(part.at[c, xc], own_ref.at[c], xsem.at[3, c]) for c in range(CHUNKS)
+    ]
+    for cp in own_copies:
+        cp.start()
     for c in range(CHUNKS):
         x_copy(0, c, part.at[c, far], xt.at[c], to_next).wait_recv()
         xsum[c] = (xt[c].astype(F32) + part[c, e_next].astype(F32)).astype(BF16)
-        start(None, x_copy(2, c, xsum.at[c], xs.at[c], to_next))
+        start(None, x_copy(2, c, xsum.at[c], summed_ref.at[c], to_next))
+    for cp in own_copies:
+        cp.wait()
     for c in range(CHUNKS):
-        x_copy(1, c, part.at[c, e_prev], xd.at[c], to_prev).wait_recv()
-        x_copy(2, c, xsum.at[c], xs.at[c], to_next).wait_recv()
-        total = part[c, xc].astype(F32) + xd[c].astype(F32) + xs[c].astype(F32)
-        mixed_ref[:, c * CHUNK : (c + 1) * CHUNK] = total.astype(BF16)
+        x_copy(1, c, part.at[c, e_prev], direct_ref.at[c], to_prev).wait_recv()
+        x_copy(2, c, xsum.at[c], summed_ref.at[c], to_next).wait_recv()
     for pred, cp in pending:
         if pred is None:
             cp.wait_send()
         else:
             pl.when(pred)(cp.wait_send)
+
+
+def finish(own_ref, direct_ref, summed_ref, lse_in, mixed_ref, lse_ref):
+    for c in range(CHUNKS):
+        total = own_ref[c].astype(F32) + direct_ref[c].astype(F32) + summed_ref[c].astype(F32)
+        mixed_ref[:, c * CHUNK : (c + 1) * CHUNK] = total.astype(BF16)
+    lse_ref[...] = lse_in[...]
 
 
 def body(*args):
@@ -484,15 +515,17 @@
         attention_output_weight, recurrence_output_weight,
     )
     dma = pltpu.SemaphoreType.DMA
-    mixed, lse = pl.pallas_call(
+    own, direct, summed, lse = pl.pallas_call(
         kernel,
         name="mixer",
         out_shape=(
-            jax.ShapeDtypeStruct((ROWS // 8, WIDTH), BF16),
+            jax.ShapeDtypeStruct((CHUNKS, ROWS // 8, CHUNK), BF16),
+            jax.ShapeDtypeStruct((CHUNKS, ROWS // 8, CHUNK), BF16),
+            jax.ShapeDtypeStruct((CHUNKS, ROWS // 8, CHUNK), BF16),
             jax.ShapeDtypeStruct((2, ROWS), F32),
         ),
         in_specs=[pl.BlockSpec(memory_space=pltpu.HBM)] * len(operands),
-        out_specs=(pl.BlockSpec(memory_space=pltpu.VMEM), pl.BlockSpec(memory_space=pltpu.VMEM)),
+        out_specs=(pl.BlockSpec(memory_space=pltpu.HBM),) * 3 + (pl.BlockSpec(memory_space=pltpu.VMEM),),
         scratch_shapes=[
             pltpu.VMEM((ROWS, WIDTH), BF16),
             pltpu.VMEM((ROWS, WIDTH), BF16),
@@ -509,6 +542,7 @@
             pltpu.VMEM((WIDTH, LANES), BF16),
             pltpu.VMEM((2 * LANES, WIDTH), BF16),
             pltpu.VMEM((2 * LANES, WIDTH), BF16),
+            pltpu.VMEM((ROWS // 2, WIDTH), F32),
             pltpu.VMEM((SHARDS, 2, ROWS), F32),
             pltpu.VMEM((2, SHARDS, ROWS, LANES), BF16),
             pltpu.VMEM((2, ROWS, LANES), BF16),
@@ -520,14 +554,14 @@
             pltpu.VMEM((ROWS, LANES), F32),
             pltpu.VMEM((ROWS, LANES), BF16),
             pltpu.VMEM((ROWS, LANES), F32),
-            pltpu.VMEM((2, ROWS // 2, 2 * LANES), BF16),
-            pltpu.VMEM((ROWS // 2, 2 * LANES), BF16),
+            pltpu.VMEM((2, ROWS // 2, LANES), BF16),
+            pltpu.VMEM((2, ROWS // 2, LANES), BF16),
+            pltpu.VMEM((ROWS // 2, LANES), BF16),
+            pltpu.VMEM((ROWS // 2, LANES), BF16),
             pltpu.VMEM((CHUNKS, RING, ROWS // 8, CHUNK), BF16),
             pltpu.VMEM((CHUNKS, ROWS // 8, CHUNK), BF16),
             pltpu.VMEM((CHUNKS, ROWS // 8, CHUNK), BF16),
-            pltpu.VMEM((CHUNKS, ROWS // 8, CHUNK), BF16),
-            pltpu.VMEM((CHUNKS, ROWS // 8, CHUNK), BF16),
-            dma((18,)),
+            dma((21,)),
             dma((SHARDS,)),
             dma((SHARDS,)),
             dma((KV_SENDS,)),
@@ -536,15 +570,23 @@
             dma((RING,)),
             dma((RING,)),
             dma((RING,)),
-            dma((2,)),
-            dma((2,)),
-            dma((3, CHUNKS)),
+            dma((4,)),
+            dma((4,)),
+            dma((4, CHUNKS)),
             dma((3, CHUNKS)),
         ],
         compiler_params=pltpu.CompilerParams(
             collective_id=0, has_side_effects=True, vmem_limit_bytes=60 * 1024 * 1024
         ),
     )(*operands)
+    mixed, lse = pl.pallas_call(
+        finish,
+        name="finish",
+        out_shape=(
+            jax.ShapeDtypeStruct((ROWS // 8, WIDTH), BF16),
+            jax.ShapeDtypeStruct((2, ROWS), F32),
+        ),
+    )(own, direct, summed, lse)
     return mixed, lse.T
 
 

time: 41.1 us -> 40.4 us (0.983); the launches traced: 40.9 us -> 39.6 us
  local copies, waits for them, and re-layouts: 2.15 us -> 0 us
  Pallas kernels: 38.1 us -> 39 us
    unnamed x4 -> x0, local copies, waits for them, and re-layouts: 2.15 us -> none
    pallas_call x1 -> x2, Pallas kernels: 38.1 us -> 39 us  [the longest x1 37.2 us: body(): pl.pallas_call(kernel, name='mixer', out_shape=(jax.ShapeDtypeStruct((CHU...]
where the time goes in v3:
time: 40.4 us; the launch traced here: 39.6 us
  Pallas kernels  39 us (97%)
  between operations  0.65 us (2%)
    pallas_call x1, Pallas kernels, body(): pl.pallas_call(kernel, name='mixer', out_shape=(jax.ShapeDtypeStruct((CHU...  37.2 us
    pallas_call x1, Pallas kernels, body(): pl.pallas_call(finish, name='finish', out_shape=(jax.ShapeDtypeStruct((RO...  1.74 us

profile of v3, /device:TPU:97, one launch (start us, length us, event | category | flops | bytes accessed | tf_op | source)
XLA Modules:
  0.0 39.6 jit_solution(17600501017697119715)
XLA Ops:
  0.6 37.2 %mixer.1 = (bf16[4,32,512]{2,1,0:T(8,128)(2,1)}, bf16[4,32,512]{2,1,0:T(8,128)(2,1)}, bf16[4,32,512]{2,1,0:T(8,128)(2,1)}, f32[2,256]{1,0:T(2,128)}) custom-call(bf16[256,2048]{1,0:T(8,128)(2,1)} %x_hbm.1, f32[1,2048]{1,0:T(1,128)} %bitcast.9, bf16[2048,128]{1,0:T(8,128)(2,1)} %wq_hbm.1, bf16[2048,128]{1,0:T(8,128)(2,1)} %wk_hbm.1, ...), custom_call_target="tpu_custom_call" | custom-call | tf_op jit(solution)/shard_map/mixer/pallas_call | solution.py:518
  37.9 1.7 %finish.1 = (bf16[32,2048]{1,0:T(8,128)(2,1)}, f32[2,256]{1,0:T(2,128)}) custom-call(bf16[4,32,512]{2,1,0:T(8,128)(2,1)} %get-tuple-element.8.own_ref, bf16[4,32,512]{2,1,0:T(8,128)(2,1)} %get-tuple-element.9.direct_ref, bf16[4,32,512]{2,1,0:T(8,128)(2,1)} %get-tuple-element.10.summed_ref, f32[2,256]{1,0:T(2,128)} %get-tuple-element.11.lse_in), custom_call_target="tpu_custom_call" | custom-call | tf_op jit(solution)/shard_map/finish/pallas_call | solution.py:582

commit v4 on v3

--- a/solution.py
+++ b/solution.py
@@ -1,3 +1,5 @@
+import functools
+
 import jax
 import jax.numpy as jnp
 from jax import lax
@@ -55,7 +57,7 @@
     gates, kv, q_v, m_v, acc_v,
     st_row, st_col, in_v, rec_v, visq_v, outgate_v,
     act_r, act_a, peer_r, peer_a, part, xt, xsum,
-    lsem, gsem, grecv, ssem, krecv, rsem, rrecv, csem, crecv, psem, precv, xsem, xrecv,
+    entered, lsem, gsem, grecv, ssem, krecv, rsem, rrecv, csem, crecv, psem, precv, xsem, xrecv,
 ):
     sp = lax.axis_index("sp")
     tp = lax.axis_index("tp")
@@ -79,12 +81,27 @@
     load("gate", gate_hbm, gates.at[sp])
 
     barrier = pltpu.get_barrier_semaphore()
-    for k in range(1, SHARDS):
-        pl.semaphore_signal(barrier, inc=1, device_id=((sp + k) % SHARDS, tp), device_id_type=MESH)
     x_right = 2 * ((xc + 1) % RING) + core
     x_left = 2 * ((xc + 3) % RING) + core
     for other in (x_right, x_left, peer):
         pl.semaphore_signal(barrier, inc=1, device_id=(sp, other), device_id_type=MESH)
+
+    def greet(k):
+        pl.semaphore_signal(barrier, inc=1, device_id=((sp + k) % SHARDS, tp), device_id_type=MESH)
+
+    def answer(k):
+        pl.semaphore_signal(entered.at[sp], inc=1, device_id=((sp + SHARDS - k) % SHARDS, tp), device_id_type=MESH)
+
+    for k in range(1, SHARDS):
+        pl.when(sp + k < SHARDS)(functools.partial(greet, k))
+    pl.semaphore_wait(barrier, sp + 3)
+    for k in (1, 4, 3, 2, 12, 5, 6, 7, 8, 9, 10, 11, 13, 14, 15):
+        pl.when(sp >= k)(functools.partial(answer, k))
+
+    def await_entry(pred, k):
+        @pl.when(pred)
+        def _():
+            pl.semaphore_wait(entered.at[(sp + k) % SHARDS], 1)
 
     pending = []
 
@@ -140,7 +157,6 @@
     kv[1, sp] = jnp.where(low, swapped, keys).astype(BF16)
 
     loads["gate"].wait()
-    pl.semaphore_wait(barrier, SHARDS - 1 + 3)
 
     y_up = z * RING + (y + 1) % RING
     y_down = z * RING + (y + 3) % RING
@@ -182,14 +198,15 @@
             device_id=(target, tp), device_id_type=MESH,
         )
 
-    for k in range(1, SHARDS):
-        target = (sp + k) % SHARDS
-        start(sp + k < SHARDS, gate_copy(sp, target))
-
-    send_along_y(None, 0, sp)
-    send_along_z(1, sp)
-    send_along_y(None, 1, sp)
-    send_along_z(0, sp)
+    await_entry(y < 3, 1)
+    send(None, 0, sp, y_up)
+    send(y > 0, 0, sp, y_down)
+    send(None, 1, sp, y_up)
+    send(y > 0, 1, sp, y_down)
+    await_entry(z < 3, RING)
+    for h in (1, 0):
+        send(z < 3, h, sp, (sp + RING) % SHARDS)
+        send((z == 1) & (core == 1), h, sp, y)
 
     loads["wf"].wait()
     loads["wrv"].wait()
@@ -232,8 +249,9 @@
             device_id=(target, tp), device_id_type=MESH,
         )
 
-    for n in range(1, RING):
-        start(None, row_copy(y, z * RING + (y + n) % RING, n))
+    await_entry(y == 0, 3)
+    send(y == 0, 0, sp, y_down)
+    send(y == 0, 1, sp, y_down)
 
     loads["wq"].wait()
     loads["wrq"].wait()
@@ -284,6 +302,13 @@
 
     attend([sp], first=True)
 
+    await_entry(z == 0, 12)
+    send(z == 0, 1, sp, 3 * RING + y)
+    send(z == 0, 0, sp, 3 * RING + y)
+    await_entry(y <= 1, 2)
+    for n in range(1, RING):
+        start(None, row_copy(y, z * RING + (y + n) % RING, n))
+
     def to_peer(n, src, dst):
         return pltpu.make_async_remote_copy(
             src_ref=src, dst_ref=dst, send_sem=psem.at[n], recv_sem=precv.at[n],
@@ -420,8 +445,18 @@
         for h, back, up in events:
             handle(h, back, up)
 
+    def share_gates():
+        later = {1: y == 3, 2: y >= 2, 3: y >= 1}
+        for k in range(1, SHARDS):
+            if k not in (RING, 12):
+                await_entry((sp + k < SHARDS) & later.get(k, True), k)
+            start(sp + k < SHARDS, gate_copy(sp, (sp + k) % SHARDS))
+
     handle_all((
         (1, 3, 0), (1, 1, 0), (0, 0, 3), (0, 0, 1), (1, 0, 1), (1, 0, 3), (0, 3, 0), (0, 3, 3), (0, 1, 0),
+    ))
+    share_gates()
+    handle_all((
         (1, 3, 1), (1, 2, 0), (1, 3, 3), (1, 1, 3), (1, 1, 1), (1, 0, 2), (0, 3, 1), (0, 0, 2), (0, 1, 1),
     ))
     attend_own_row()
@@ -432,11 +467,8 @@
     handle_all(((0, 1, 2), (1, 1, 2), (0, 2, 1)))
     attend_row(1, (0, 1, 3, 2))
     share_recurrence()
-    handle_all(((0, 2, 3),))
-    project_recurrence()
-    handle_all(((0, 2, 2), (1, 2, 2)))
+    handle_all(((0, 2, 3), (0, 2, 2), (1, 2, 2)))
     attend_row(2, (0, 1, 3, 2))
-
     a0, a1 = acc_v[0], acc_v[1]
     totals = jnp.where(low, a0, a1)
     loads["ag"].wait()
@@ -448,20 +480,27 @@
     log_sum = (jnp.where(low, m_v[0], m_v[1]) + jnp.log(totals)).T
     lse_ref[0:1, :] = log_sum[0:1, :] + gates[sp, 0:1, :]
     lse_ref[1:2, :] = log_sum[HALF : HALF + 1, :] + gates[sp, 1:2, :]
+    project_recurrence()
     woa_copy.wait_recv()
     act_copy.wait_recv()
 
-    e_next = (xc + 2 * core + 3) % RING
-    e_prev = (xc + 5 - 2 * core) % RING
     far = (xc + 2) % RING
-    to_next = 2 * e_next + core
-    to_prev = 2 * e_prev + core
+    sides = ((xc + 3) % RING, (xc + 1) % RING)
 
     def x_copy(kind, c, src, dst, target):
         return pltpu.make_async_remote_copy(
             src_ref=src, dst_ref=dst, send_sem=xsem.at[kind, c], recv_sem=xrecv.at[kind, c],
             device_id=(sp, target), device_id_type=MESH,
         )
+
+    def transit(c):
+        return x_copy(0, c, part.at[c, far], xt.at[c], 2 * sides[c % 2] + core)
+
+    def direct(c):
+        return x_copy(1, c, part.at[c, sides[1 - c % 2]], direct_ref.at[c], 2 * sides[1 - c % 2] + core)
+
+    def summed(c):
+        return x_copy(2, c, xsum.at[c], summed_ref.at[c], 2 * sides[c % 2] + core)
 
     both = jnp.concatenate([act_a[core], peer_a[...]], axis=1)
     for c in range(CHUNKS):
@@ -469,23 +508,23 @@
         product = product_v[:, cols] + dot(both, woa[:, cols])
         for b in range(RING):
             part[c, b] = product[32 * b : 32 * b + 32].astype(BF16)
-        start(None, x_copy(0, c, part.at[c, far], xt.at[c], to_next))
+        start(None, transit(c))
     for c in range(CHUNKS):
-        start(None, x_copy(1, c, part.at[c, e_prev], direct_ref.at[c], to_prev))
+        start(None, direct(c))
     own_copies = [
         pltpu.make_async_copy(part.at[c, xc], own_ref.at[c], xsem.at[3, c]) for c in range(CHUNKS)
     ]
     for cp in own_copies:
         cp.start()
     for c in range(CHUNKS):
-        x_copy(0, c, part.at[c, far], xt.at[c], to_next).wait_recv()
-        xsum[c] = (xt[c].astype(F32) + part[c, e_next].astype(F32)).astype(BF16)
-        start(None, x_copy(2, c, xsum.at[c], summed_ref.at[c], to_next))
+        transit(c).wait_recv()
+        xsum[c] = (xt[c].astype(F32) + part[c, sides[c % 2]].astype(F32)).astype(BF16)
+        start(None, summed(c))
     for cp in own_copies:
         cp.wait()
     for c in range(CHUNKS):
-        x_copy(1, c, part.at[c, e_prev], direct_ref.at[c], to_prev).wait_recv()
-        x_copy(2, c, xsum.at[c], summed_ref.at[c], to_next).wait_recv()
+        direct(c).wait_recv()
+        summed(c).wait_recv()
     for pred, cp in pending:
         if pred is None:
             cp.wait_send()
@@ -561,6 +600,7 @@
             pltpu.VMEM((CHUNKS, RING, ROWS // 8, CHUNK), BF16),
             pltpu.VMEM((CHUNKS, ROWS // 8, CHUNK), BF16),
             pltpu.VMEM((CHUNKS, ROWS // 8, CHUNK), BF16),
+            pltpu.SemaphoreType.REGULAR((SHARDS,)),
             dma((21,)),
             dma((SHARDS,)),
             dma((SHARDS,)),

time: 40.4 us -> 38.9 us (0.963); the launches traced: 39.6 us -> 38.8 us
  Pallas kernels: 39 us -> 38.1 us
    pallas_call x1, Pallas kernels: 37.2 us -> 36.4 us  [body(): pl.pallas_call(kernel, name='mixer', out_shape=(jax.ShapeDtypeStruct((CHU...]
where the time goes in v4:
time: 38.9 us; the launch traced here: 38.8 us
  Pallas kernels  38.1 us (98%)
  between operations  0.65 us (2%)
    pallas_call x1, Pallas kernels, body(): pl.pallas_call(kernel, name='mixer', out_shape=(jax.ShapeDtypeStruct((CHU...  36.4 us
    pallas_call x1, Pallas kernels, body(): pl.pallas_call(finish, name='finish', out_shape=(jax.ShapeDtypeStruct((RO...  1.74 us

profile of v4, /device:TPU:97, one launch (start us, length us, event | category | flops | bytes accessed | tf_op | source)
XLA Modules:
  0.0 38.8 jit_solution(177169580233835750)
XLA Ops:
  0.6 36.4 %mixer.1 = (bf16[4,32,512]{2,1,0:T(8,128)(2,1)}, bf16[4,32,512]{2,1,0:T(8,128)(2,1)}, bf16[4,32,512]{2,1,0:T(8,128)(2,1)}, f32[2,256]{1,0:T(2,128)}) custom-call(bf16[256,2048]{1,0:T(8,128)(2,1)} %x_hbm.1, f32[1,2048]{1,0:T(1,128)} %bitcast.9, bf16[2048,128]{1,0:T(8,128)(2,1)} %wq_hbm.1, bf16[2048,128]{1,0:T(8,128)(2,1)} %wk_hbm.1, ...), custom_call_target="tpu_custom_call" | custom-call | tf_op jit(solution)/shard_map/mixer/pallas_call | solution.py:557
  37.0 1.7 %finish.1 = (bf16[32,2048]{1,0:T(8,128)(2,1)}, f32[2,256]{1,0:T(2,128)}) custom-call(bf16[4,32,512]{2,1,0:T(8,128)(2,1)} %get-tuple-element.8.own_ref, bf16[4,32,512]{2,1,0:T(8,128)(2,1)} %get-tuple-element.9.direct_ref, bf16[4,32,512]{2,1,0:T(8,128)(2,1)} %get-tuple-element.10.summed_ref, f32[2,256]{1,0:T(2,128)} %get-tuple-element.11.lse_in), custom_call_target="tpu_custom_call" | custom-call | tf_op jit(solution)/shard_map/finish/pallas_call | solution.py:622

commit v5 on v4

--- a/solution.py
+++ b/solution.py
@@ -51,12 +51,12 @@
 def kernel(
     x_hbm, xg_hbm, wq_hbm, wk_hbm, wv_hbm, qg_hbm, kg_hbm, gate_hbm, ag_hbm,
     wrq_hbm, wf_hbm, wrv_hbm, wog_hbm, slack_hbm, extra_hbm, rg_hbm, woa_hbm, wor_hbm,
-    own_ref, direct_ref, summed_ref, lse_ref,
+    mixed_ref, lse_ref,
     x_v, n_v, xg_v, qg_v, kg_v, ag_v, slack_v, extra_v, rg_v,
     wkv, wfr, wqq, wog, woa, wor, product_v,
     gates, kv, q_v, m_v, acc_v,
     st_row, st_col, in_v, rec_v, visq_v, outgate_v,
-    act_r, act_a, peer_r, peer_a, part, xt, xsum,
+    act_r, act_a, peer_r, peer_a, part, xt, near, relayed, xsum,
     entered, lsem, gsem, grecv, ssem, krecv, rsem, rrecv, csem, crecv, psem, precv, xsem, xrecv,
 ):
     sp = lax.axis_index("sp")
@@ -81,27 +81,49 @@
     load("gate", gate_hbm, gates.at[sp])
 
     barrier = pltpu.get_barrier_semaphore()
-    x_right = 2 * ((xc + 1) % RING) + core
-    x_left = 2 * ((xc + 3) % RING) + core
-    for other in (x_right, x_left, peer):
-        pl.semaphore_signal(barrier, inc=1, device_id=(sp, other), device_id_type=MESH)
-
-    def greet(k):
-        pl.semaphore_signal(barrier, inc=1, device_id=((sp + k) % SHARDS, tp), device_id_type=MESH)
-
-    def answer(k):
-        pl.semaphore_signal(entered.at[sp], inc=1, device_id=((sp + SHARDS - k) % SHARDS, tp), device_id_type=MESH)
-
-    for k in range(1, SHARDS):
-        pl.when(sp + k < SHARDS)(functools.partial(greet, k))
-    pl.semaphore_wait(barrier, sp + 3)
-    for k in (1, 4, 3, 2, 12, 5, 6, 7, 8, 9, 10, 11, 13, 14, 15):
-        pl.when(sp >= k)(functools.partial(answer, k))
-
-    def await_entry(pred, k):
+
+    def along_y(k):
+        return (z * RING + (y + k) % RING, tp)
+
+    def along_z(k):
+        return ((sp + RING * k) % SHARDS, tp)
+
+    def along_x(k):
+        return (sp, 2 * ((xc + k) % RING) + core)
+
+    def greet(pred, device):
         @pl.when(pred)
         def _():
-            pl.semaphore_wait(entered.at[(sp + k) % SHARDS], 1)
+            pl.semaphore_signal(barrier, inc=1, device_id=device, device_id_type=MESH)
+
+    def answer(pred, kind, k, device):
+        @pl.when(pred)
+        def _():
+            pl.semaphore_signal(entered.at[kind, k], inc=1, device_id=device, device_id_type=MESH)
+
+    def await_entry(pred, kind, k):
+        @pl.when(pred)
+        def _():
+            pl.semaphore_wait(entered.at[kind, k], 1)
+
+    for k in range(1, RING):
+        greet(y + k < RING, along_y(k))
+        greet(z + k < RING, along_z(k))
+    greet(xc < 3, along_x(1))
+    greet(xc == 0, along_x(3))
+    greet(core == 0, (sp, peer))
+    earlier = y + z + (xc + 3) // 4 + xc // 3 + core
+
+    @pl.when(earlier > 0)
+    def _():
+        pl.semaphore_wait(barrier, earlier)
+
+    for k in range(1, RING):
+        answer(y >= k, 0, k, along_y(RING - k))
+        answer(z >= k, 1, k, along_z(RING - k))
+    answer(core == 1, 2, 0, (sp, peer))
+    answer(xc > 0, 2, 1, along_x(3))
+    answer(xc == 3, 2, 3, along_x(1))
 
     pending = []
 
@@ -192,40 +214,21 @@
         send(pred, h, j, y_up)
         send(pred, h, j, y_down)
 
-    def gate_copy(j, target):
+    def gate_copy(j, k):
         return pltpu.make_async_remote_copy(
-            src_ref=gates.at[j], dst_ref=gates.at[j], send_sem=gsem.at[target], recv_sem=grecv.at[j],
-            device_id=(target, tp), device_id_type=MESH,
+            src_ref=gates.at[j], dst_ref=gates.at[j], send_sem=gsem.at[0, k], recv_sem=grecv.at[0, j % RING],
+            device_id=along_y(k), device_id_type=MESH,
         )
 
-    await_entry(y < 3, 1)
-    send(None, 0, sp, y_up)
-    send(y > 0, 0, sp, y_down)
-    send(None, 1, sp, y_up)
-    send(y > 0, 1, sp, y_down)
-    await_entry(z < 3, RING)
-    for h in (1, 0):
-        send(z < 3, h, sp, (sp + RING) % SHARDS)
-        send((z == 1) & (core == 1), h, sp, y)
-
-    loads["wf"].wait()
-    loads["wrv"].wait()
-    loads["slack"].wait()
-    loads["extra"].wait()
-    fr = dot(n_v[...], wfr[...])
-    forget = slack_v[...] * (1.0 / (1.0 + jnp.exp(fr[:, :LANES])))
-    rec_value = fr[:, LANES:].astype(BF16)
-    extra = jnp.broadcast_to(extra_v[...], (LANES, ROWS)).T
+    def gate_rows(row, k):
+        four = gates.at[pl.ds(row * RING, RING)]
+        return pltpu.make_async_remote_copy(
+            src_ref=four, dst_ref=four, send_sem=gsem.at[1, k], recv_sem=grecv.at[1, row],
+            device_id=along_z(k), device_id_type=MESH,
+        )
+
     row_at, col_at = iota((ROWS, ROWS), 0), iota((ROWS, ROWS), 1)
     causal = col_at <= row_at
-    lower = jnp.where(causal, 1.0, 0.0).astype(BF16)
-    sums = dot(lower, jnp.concatenate(split3(jnp.log1p(-forget)) + split3(extra), axis=1))
-    share_sum = sums[:, :LANES] + sums[:, LANES : 2 * LANES] + sums[:, 2 * LANES : 3 * LANES]
-    extra_sum = sums[:, 3 * LANES : 4 * LANES] + sums[:, 4 * LANES : 5 * LANES] + sums[:, 5 * LANES :]
-    share_end = share_sum[ROWS - 1 :, :]
-    extra_end = extra_sum[ROWS - 1 :, :]
-    closing = (forget * jnp.exp((share_end - share_sum) + (extra_end - extra_sum))).astype(BF16)
-    state_t = dot(fr[:, LANES:].T.astype(BF16), closing)
 
     def state_message(state, decay):
         hi, mid, lo = (part.astype(F32) for part in split3(decay))
@@ -233,10 +236,6 @@
         tail = jnp.where(at == 0, hi, jnp.where(at == 1, mid, jnp.where(at == 2, lo, 0.0)))
         return state.astype(BF16), tail.astype(BF16)
 
-    body, tail = state_message(state_t, share_end + extra_end)
-    st_row[y, :LANES] = body
-    st_row[y, LANES:] = tail
-
     def row_copy(j, target, n):
         return pltpu.make_async_remote_copy(
             src_ref=st_row.at[j], dst_ref=st_row.at[j], send_sem=rsem.at[n], recv_sem=rrecv.at[j],
@@ -249,38 +248,95 @@
             device_id=(target, tp), device_id_type=MESH,
         )
 
-    await_entry(y == 0, 3)
-    send(y == 0, 0, sp, y_down)
-    send(y == 0, 1, sp, y_down)
-
-    loads["wq"].wait()
-    loads["wrq"].wait()
-    loads["qg"].wait()
-    qq = dot(n_v[...], wqq[...])
-    queries = (half_rms(qq[:, :LANES], twice(qg_v[...])).astype(BF16).astype(F32)) * (HALF**-0.5)
-    q_v[0] = jnp.where(low, queries, 0.0).astype(BF16)
-    q_v[1] = jnp.where(low, 0.0, queries).astype(BF16)
-
-    rq = qq[:, LANES:]
-    rec_query = rq / (1.0 + jnp.exp(-rq))
-    scores = dot_nt((rec_query * jnp.exp(share_sum)).astype(BF16), (forget * jnp.exp(-share_sum)).astype(BF16))
-    differ = jnp.concatenate([extra_sum, extra_sum], axis=1) - extra_sum.T[:1, :]
-    scores = scores * jnp.exp(jnp.where(causal, differ, NEGATIVE))
-    rec_v[...] = dot(scores.astype(BF16), rec_value)
-    visq_v[...] = (rec_query * jnp.exp(share_sum + extra_sum)).astype(BF16)
-
-    loads["wog"].wait()
-    og = dot(n_v[...], wog[...])
-    outgate_v[...] = og / (1.0 + jnp.exp(-og))
+    def first_y():
+        await_entry(y < 3, 0, 1)
+        send((y < 3) | (z < 3), 0, sp, y_up)
+        send((y > 0) & (z < 3), 0, sp, y_down)
+        send(y < 3, 1, sp, y_up)
+        send((y == 1) & (core == 1), 1, sp, y_down)
+        send((y == 1) & (core == 1) & (z == 3), 0, sp, y_down)
+
+    def first_z():
+        await_entry(z < 3, 1, 1)
+        for h in (1, 0):
+            send(z < 3, h, sp, (sp + RING) % SHARDS)
+            send((z == 1) & (core == 1), h, sp, y)
+
+    def last_y():
+        await_entry(y == 0, 0, 3)
+        send(y == 0, 0, sp, y_down)
+        send(y == 0, 1, sp, y_down)
+
+    def last_z():
+        await_entry(z == 0, 1, 3)
+        for h in (1, 0):
+            send(z == 0, h, sp, 3 * RING + y)
+
+    def share_row_gates():
+        await_entry(y <= 1, 0, 2)
+        for k in range(1, RING):
+            start(None, gate_copy(sp, k))
+
+    def share_states():
+        for n in range(1, RING):
+            start(None, row_copy(y, z * RING + (y + n) % RING, n))
+
+    def recurrence():
+        loads["wf"].wait()
+        loads["wrv"].wait()
+        loads["slack"].wait()
+        loads["extra"].wait()
+        fr = dot(n_v[...], wfr[...])
+        forget = slack_v[...] * (1.0 / (1.0 + jnp.exp(fr[:, :LANES])))
+        rec_value = fr[:, LANES:].astype(BF16)
+        extra = jnp.broadcast_to(extra_v[...], (LANES, ROWS)).T
+        lower_tri = jnp.where(causal, 1.0, 0.0).astype(BF16)
+        sums = dot(lower_tri, jnp.concatenate(split3(jnp.log1p(-forget)) + split3(extra), axis=1))
+        share_sum = sums[:, :LANES] + sums[:, LANES : 2 * LANES] + sums[:, 2 * LANES : 3 * LANES]
+        extra_sum = sums[:, 3 * LANES : 4 * LANES] + sums[:, 4 * LANES : 5 * LANES] + sums[:, 5 * LANES :]
+        share_end = share_sum[ROWS - 1 :, :]
+        extra_end = extra_sum[ROWS - 1 :, :]
+        closing = (forget * jnp.exp((share_end - share_sum) + (extra_end - extra_sum))).astype(BF16)
+        state_t = dot(fr[:, LANES:].T.astype(BF16), closing)
+
+        body, tail = state_message(state_t, share_end + extra_end)
+        st_row[y, :LANES] = body
+        st_row[y, LANES:] = tail
+        return forget, rec_value, share_sum, extra_sum
+
+    def query_side(forget, rec_value, share_sum, extra_sum):
+        loads["wq"].wait()
+        loads["wrq"].wait()
+        loads["qg"].wait()
+        qq = dot(n_v[...], wqq[...])
+        queries = (half_rms(qq[:, :LANES], twice(qg_v[...])).astype(BF16).astype(F32)) * (HALF**-0.5)
+        q_v[0] = jnp.where(low, queries, 0.0).astype(BF16)
+        q_v[1] = jnp.where(low, 0.0, queries).astype(BF16)
+
+        rq = qq[:, LANES:]
+        rec_query = rq / (1.0 + jnp.exp(-rq))
+        scores = dot_nt((rec_query * jnp.exp(share_sum)).astype(BF16), (forget * jnp.exp(-share_sum)).astype(BF16))
+        differ = jnp.concatenate([extra_sum, extra_sum], axis=1) - extra_sum.T[:1, :]
+        scores = scores * jnp.exp(jnp.where(causal, differ, NEGATIVE))
+        rec_v[...] = dot(scores.astype(BF16), rec_value)
+        visq_v[...] = (rec_query * jnp.exp(share_sum + extra_sum)).astype(BF16)
+
+        loads["wog"].wait()
+        og = dot(n_v[...], wog[...])
+        outgate_v[...] = og / (1.0 + jnp.exp(-og))
 
     def attend(blocks, first=False, shown=None):
+        def keys_of(h, i, j):
+            block = kv[h, j]
+            return block if shown is None or shown[i] is None else jnp.where(shown[i], block, jnp.zeros_like(block))
+
         for h in range(2):
             parts = []
             for i, j in enumerate(blocks):
                 gate = gates[j, h : h + 1, :]
-                if shown is not None:
+                if shown is not None and shown[i] is not None:
                     gate = jnp.where(shown[i], gate, -NEGATIVE)
-                part = dot_nt(q_v[h], kv[h, j]) - gate
+                part = dot_nt(q_v[h], keys_of(h, i, j)) - gate
                 parts.append(jnp.where(causal, part, NEGATIVE) if first else part)
             widest = parts[0]
             for part in parts[1:]:
@@ -290,9 +346,9 @@
                 old = m_v[h]
                 top = jnp.maximum(old[:, :1], top)
             summed = None if first else acc_v[h] * jnp.exp(old - top)
-            for part, j in zip(parts, blocks):
+            for i, (part, j) in enumerate(zip(parts, blocks)):
                 weights = jnp.exp(part - top).astype(BF16)
-                block = kv[h, j]
+                block = keys_of(h, i, j)
                 ones = jnp.ones_like(block)
                 right = jnp.where(low, ones, block) if h == 0 else jnp.where(low, block, ones)
                 term = dot(weights, right)
@@ -300,36 +356,20 @@
             acc_v[h] = summed
             m_v[h] = jnp.broadcast_to(top, (ROWS, LANES))
 
-    attend([sp], first=True)
-
-    await_entry(z == 0, 12)
-    send(z == 0, 1, sp, 3 * RING + y)
-    send(z == 0, 0, sp, 3 * RING + y)
-    await_entry(y <= 1, 2)
-    for n in range(1, RING):
-        start(None, row_copy(y, z * RING + (y + n) % RING, n))
-
     def to_peer(n, src, dst):
         return pltpu.make_async_remote_copy(
             src_ref=src, dst_ref=dst, send_sem=psem.at[n], recv_sem=precv.at[n],
             device_id=(sp, peer), device_id_type=MESH,
         )
 
-    loads["woa"].wait()
-    loads["wor"].wait()
     wor_copy = to_peer(0, wor.at[pl.ds(0, LANES)], wor.at[pl.ds(LANES, LANES)])
     woa_copy = to_peer(1, woa.at[pl.ds(0, LANES)], woa.at[pl.ds(LANES, LANES)])
-    start(None, wor_copy)
-    start(None, woa_copy)
-
-    def wait_gate(valid, j):
-        pl.when(valid)(gate_copy(j, j).wait_recv)
-
-    hops = {0: 0, 1: 1, 3: 1, 2: 2}
-    plan = sorted(
-        ((back, up) for back in (0, 1, 3, 2) for up in (0, 1, 3, 2) if (back, up) != (0, 0)),
-        key=lambda e: hops[e[0]] + hops[e[1]],
-    )
+    def share_weights():
+        loads["woa"].wait()
+        loads["wor"].wait()
+        await_entry(core == 0, 2, 0)
+        start(None, wor_copy)
+        start(None, woa_copy)
 
     def shard_of(back, up):
         return ((z + RING - back) % RING) * RING + (y + up) % RING
@@ -341,49 +381,53 @@
             send((z == 3) & (core == 1), h, j, 2 * RING + y)
 
     def handle(h, back, up):
-        valid = None if back == 0 else z >= back
         j = shard_of(back, up)
+        if back == 0:
+            wanted = y + up >= RING
+            if up == 1:
+                wanted = wanted | (y == 0) & (core == 1)
+            arrive(wanted if h else wanted | (z < 3), h, j)
+            if up == 3:
+                onward = (core == 0) & ((y == 1) | (y == 2))
+                send(onward if h else onward | (core == 0) & (z < 3), h, j, y_up)
+            if up == 1:
+                onward = (core == 1) & ((y == 3) | (y == 0))
+                send(onward if h else onward | (core == 1) & (z < 3), h, j, y_down)
+            if h == 0:
+                send_along_z(h, j)
+            return
+        valid = z >= back
         arrive(valid, h, j)
         if h == 0:
-            if back == 0:
-                if up == 3:
-                    send(core == 0, h, j, y_up)
-                if up == 1:
-                    send(core == 1, h, j, y_down)
-                send_along_z(h, j)
-            else:
-                relay_z(valid, h, j, back)
-        else:
-            if up == 0:
-                relay_z(valid, h, j, back)
-                send_along_y(valid, h, j)
-            else:
-                fine = core == (0 if up == 3 else 1)
-                if up != 2:
-                    send(fine if valid is None else fine & valid, h, j, y_up if up == 3 else y_down)
+            relay_z(valid, h, j, back)
+        elif up == 0:
+            relay_z(valid, h, j, back)
+            send_along_y(valid, h, j)
+        elif up == 3:
+            send((core == 0) & valid, h, j, y_up)
+        elif up == 1:
+            send((core == 1) & valid, h, j, y_down)
         if back == 1 and (h == 0 or up == 0):
             through = (z == 0) & (core == 1)
             jj = RING + (y + up) % RING
             arrive(through, h, jj)
             send(through, h, jj, 3 * RING + y)
 
-    def attend_own_row():
-        blocks = [shard_of(0, up) for up in (1, 2, 3)]
-        shown = [y + up >= RING for up in (1, 2, 3)]
-        for valid, j in zip(shown, blocks):
-            wait_gate(valid, j)
-
-        @pl.when(y > 0)
-        def _():
-            attend(blocks, shown=shown)
-
-    def attend_row(back, ups):
-        @pl.when(z >= back)
-        def _():
-            blocks = [shard_of(back, up) for up in ups]
-            for j in blocks:
-                gate_copy(j, j).wait_recv()
-            attend(blocks)
+    def attend_rows(backs):
+        for at in range(RING):
+            rows = [b for b in backs if b <= at]
+
+            @pl.when((z == at) & (y > 0) if rows == [0] else z == at)
+            def _():
+                blocks, shown = [], []
+                for b in rows:
+                    for up in (1, 2, 3) if b == 0 else (0, 1, 3, 2):
+                        blocks.append(shard_of(b, up))
+                        shown.append(y + up >= RING if b == 0 else None)
+                    if b > 0:
+                        gate_rows((z + RING - b) % RING, b).wait_recv()
+                if blocks:
+                    attend(blocks, shown=shown)
 
     def read_state(ref, j):
         tail = ref[j, LANES:].astype(F32)
@@ -446,29 +490,57 @@
             handle(h, back, up)
 
     def share_gates():
-        later = {1: y == 3, 2: y >= 2, 3: y >= 1}
-        for k in range(1, SHARDS):
-            if k not in (RING, 12):
-                await_entry((sp + k < SHARDS) & later.get(k, True), k)
-            start(sp + k < SHARDS, gate_copy(sp, (sp + k) % SHARDS))
-
-    handle_all((
-        (1, 3, 0), (1, 1, 0), (0, 0, 3), (0, 0, 1), (1, 0, 1), (1, 0, 3), (0, 3, 0), (0, 3, 3), (0, 1, 0),
+        await_entry(z <= 1, 1, 2)
+        for k in range(1, RING):
+            gate_copy(z * RING + (y + k) % RING, k).wait_recv()
+        for k in range(1, RING):
+            start(z + k < RING, gate_rows(z, k))
+
+    first_y()
+    last_y()
+    share_row_gates()
+    first_z()
+    local = recurrence()
+    share_states()
+    last_z()
+    handle_all((
+        (1, 3, 0), (1, 1, 0), (0, 0, 3), (0, 0, 1),
+    ))
+    query_side(*local)
+    handle_all((
+        (0, 3, 0), (1, 2, 0), (1, 0, 1), (0, 1, 0),
+    ))
+    share_weights()
+    handle_all((
+        (0, 3, 3), (1, 3, 3),
+    ))
+    attend([sp], first=True)
+    handle_all((
+        (0, 1, 3),
     ))
     share_gates()
     handle_all((
-        (1, 3, 1), (1, 2, 0), (1, 3, 3), (1, 1, 3), (1, 1, 1), (1, 0, 2), (0, 3, 1), (0, 0, 2), (0, 1, 1),
-    ))
-    attend_own_row()
-    handle_all(((0, 2, 0), (1, 2, 3), (0, 1, 3)))
+        (0, 3, 1), (1, 0, 3), (1, 1, 3), (0, 0, 2),
+    ))
     combine_row()
-    handle_all(((0, 3, 2), (1, 2, 1), (1, 3, 2)))
-    attend_row(3, (0, 1, 3, 2))
-    handle_all(((0, 1, 2), (1, 1, 2), (0, 2, 1)))
-    attend_row(1, (0, 1, 3, 2))
+    handle_all((
+        (1, 3, 1), (1, 1, 1), (0, 2, 0), (1, 2, 3), (1, 2, 1), (0, 1, 2), (1, 0, 2),
+    ))
+    attend_rows((0,))
+    handle_all((
+        (0, 1, 1), (0, 3, 2), (1, 3, 2),
+    ))
+    attend_rows((3,))
+    handle_all((
+        (1, 1, 2),
+    ))
+    attend_rows((1,))
     share_recurrence()
-    handle_all(((0, 2, 3), (0, 2, 2), (1, 2, 2)))
-    attend_row(2, (0, 1, 3, 2))
+    handle_all((
+        (1, 2, 2), (0, 2, 3), (0, 2, 1), (0, 2, 2),
+    ))
+    attend_rows((2,))
+
     a0, a1 = acc_v[0], acc_v[1]
     totals = jnp.where(low, a0, a1)
     loads["ag"].wait()
@@ -480,6 +552,8 @@
     log_sum = (jnp.where(low, m_v[0], m_v[1]) + jnp.log(totals)).T
     lse_ref[0:1, :] = log_sum[0:1, :] + gates[sp, 0:1, :]
     lse_ref[1:2, :] = log_sum[HALF : HALF + 1, :] + gates[sp, 1:2, :]
+    await_entry(xc < 3, 2, 1)
+    await_entry(xc == 0, 2, 3)
     project_recurrence()
     woa_copy.wait_recv()
     act_copy.wait_recv()
@@ -497,10 +571,10 @@
         return x_copy(0, c, part.at[c, far], xt.at[c], 2 * sides[c % 2] + core)
 
     def direct(c):
-        return x_copy(1, c, part.at[c, sides[1 - c % 2]], direct_ref.at[c], 2 * sides[1 - c % 2] + core)
+        return x_copy(1, c, part.at[c, sides[1 - c % 2]], near.at[c], 2 * sides[1 - c % 2] + core)
 
     def summed(c):
-        return x_copy(2, c, xsum.at[c], summed_ref.at[c], 2 * sides[c % 2] + core)
+        return x_copy(2, c, xsum.at[c], relayed.at[c], 2 * sides[c % 2] + core)
 
     both = jnp.concatenate([act_a[core], peer_a[...]], axis=1)
     for c in range(CHUNKS):
@@ -511,20 +585,15 @@
         start(None, transit(c))
     for c in range(CHUNKS):
         start(None, direct(c))
-    own_copies = [
-        pltpu.make_async_copy(part.at[c, xc], own_ref.at[c], xsem.at[3, c]) for c in range(CHUNKS)
-    ]
-    for cp in own_copies:
-        cp.start()
     for c in range(CHUNKS):
         transit(c).wait_recv()
         xsum[c] = (xt[c].astype(F32) + part[c, sides[c % 2]].astype(F32)).astype(BF16)
         start(None, summed(c))
-    for cp in own_copies:
-        cp.wait()
     for c in range(CHUNKS):
         direct(c).wait_recv()
         summed(c).wait_recv()
+        total = part[c, xc].astype(F32) + near[c].astype(F32) + relayed[c].astype(F32)
+        mixed_ref[:, c * CHUNK : (c + 1) * CHUNK] = total.astype(BF16)
     for pred, cp in pending:
         if pred is None:
             cp.wait_send()
@@ -532,11 +601,15 @@
             pl.when(pred)(cp.wait_send)
 
 
-def finish(own_ref, direct_ref, summed_ref, lse_in, mixed_ref, lse_ref):
-    for c in range(CHUNKS):
-        total = own_ref[c].astype(F32) + direct_ref[c].astype(F32) + summed_ref[c].astype(F32)
-        mixed_ref[:, c * CHUNK : (c + 1) * CHUNK] = total.astype(BF16)
-    lse_ref[...] = lse_in[...]
+def finish(mixed_v, lse_v, mixed_hbm, lse_hbm, sem):
+    copies = [
+        pltpu.make_async_copy(mixed_v, mixed_hbm, sem.at[0]),
+        pltpu.make_async_copy(lse_v, lse_hbm, sem.at[1]),
+    ]
+    for cp in copies:
+        cp.start()
+    for cp in copies:
+        cp.wait()
 
 
 def body(*args):
@@ -553,18 +626,17 @@
         gate_lower_slack[None], extra_log_decay.T, recurrence_norm_gain[None],
         attention_output_weight, recurrence_output_weight,
     )
+    operands = [pltpu.with_memory_space_constraint(a, pltpu.HBM) for a in operands]
     dma = pltpu.SemaphoreType.DMA
-    own, direct, summed, lse = pl.pallas_call(
+    mixed, lse = pl.pallas_call(
         kernel,
         name="mixer",
         out_shape=(
-            jax.ShapeDtypeStruct((CHUNKS, ROWS // 8, CHUNK), BF16),
-            jax.ShapeDtypeStruct((CHUNKS, ROWS // 8, CHUNK), BF16),
-            jax.ShapeDtypeStruct((CHUNKS, ROWS // 8, CHUNK), BF16),
-            jax.ShapeDtypeStruct((2, ROWS), F32),
+            pltpu.VMEM((ROWS // 8, WIDTH), BF16),
+            pltpu.VMEM((2, ROWS), F32),
         ),
         in_specs=[pl.BlockSpec(memory_space=pltpu.HBM)] * len(operands),
-        out_specs=(pl.BlockSpec(memory_space=pltpu.HBM),) * 3 + (pl.BlockSpec(memory_space=pltpu.VMEM),),
+        out_specs=(pl.BlockSpec(memory_space=pltpu.VMEM),) * 2,
         scratch_shapes=[
             pltpu.VMEM((ROWS, WIDTH), BF16),
             pltpu.VMEM((ROWS, WIDTH), BF16),
@@ -600,10 +672,12 @@
             pltpu.VMEM((CHUNKS, RING, ROWS // 8, CHUNK), BF16),
             pltpu.VMEM((CHUNKS, ROWS // 8, CHUNK), BF16),
             pltpu.VMEM((CHUNKS, ROWS // 8, CHUNK), BF16),
-            pltpu.SemaphoreType.REGULAR((SHARDS,)),
+            pltpu.VMEM((CHUNKS, ROWS // 8, CHUNK), BF16),
+            pltpu.VMEM((CHUNKS, ROWS // 8, CHUNK), BF16),
+            pltpu.SemaphoreType.REGULAR((3, RING)),
             dma((21,)),
-            dma((SHARDS,)),
-            dma((SHARDS,)),
+            dma((2, RING)),
+            dma((2, RING)),
             dma((KV_SENDS,)),
             dma((2, SHARDS)),
             dma((RING,)),
@@ -612,11 +686,11 @@
             dma((RING,)),
             dma((4,)),
             dma((4,)),
-            dma((4, CHUNKS)),
+            dma((3, CHUNKS)),
             dma((3, CHUNKS)),
         ],
         compiler_params=pltpu.CompilerParams(
-            collective_id=0, has_side_effects=True, vmem_limit_bytes=60 * 1024 * 1024
+            collective_id=0, has_side_effects=True, vmem_limit_bytes=40 * 1024 * 1024
         ),
     )(*operands)
     mixed, lse = pl.pallas_call(
@@ -626,7 +700,10 @@
             jax.ShapeDtypeStruct((ROWS // 8, WIDTH), BF16),
             jax.ShapeDtypeStruct((2, ROWS), F32),
         ),
-    )(own, direct, summed, lse)
+        in_specs=[pl.BlockSpec(memory_space=pltpu.VMEM)] * 2,
+        out_specs=(pl.BlockSpec(memory_space=pltpu.HBM),) * 2,
+        scratch_shapes=[pltpu.SemaphoreType.DMA((2,))],
+    )(pltpu.with_memory_space_constraint(mixed, pltpu.VMEM), pltpu.with_memory_space_constraint(lse, pltpu.VMEM))
     return mixed, lse.T
 
 

time: 38.9 us -> 34.3 us (0.88)
  Pallas kernels: 38.1 us -> 33.1 us
    pallas_call x1, Pallas kernels: 36.4 us -> 32.4 us  [body(): pl.pallas_call(kernel, name='mixer', out_shape=(pltpu.VMEM((ROWS // 8, WI...]
    pallas_call x1, Pallas kernels: 1.74 us -> 0.68 us  [body(): pl.pallas_call(finish, name='finish', out_shape=(jax.ShapeDtypeStruct((RO...]
where the time goes in v5:
time: 34.3 us; the launch traced here: 33.9 us
  Pallas kernels  33.1 us (97%)
  between operations  0.81 us (2%)
    pallas_call x1, Pallas kernels, body(): pl.pallas_call(kernel, name='mixer', out_shape=(pltpu.VMEM((ROWS // 8, WI...  32.4 us

profile of v5, /device:TPU:97, one launch (start us, length us, event | category | flops | bytes accessed | tf_op | source)
XLA Modules:
  0.0 33.9 jit_solution(15726225838755852864)
XLA Ops:
  0.6 32.4 %mixer.1 = (bf16[32,2048]{1,0:T(8,128)(2,1)S(1)}, f32[2,256]{1,0:T(2,128)S(1)}) custom-call(bf16[256,2048]{1,0:T(8,128)(2,1)} %x_hbm.1, f32[1,2048]{1,0:T(1,128)} %bitcast.9, bf16[2048,128]{1,0:T(8,128)(2,1)} %wq_hbm.1, bf16[2048,128]{1,0:T(8,128)(2,1)} %wk_hbm.1, bf16[2048,128]{1,0:T(8,128)(2,1)} %wv_hbm.1, f32[1,64]{1,0:T(1,128)} %bitcast.12, ...), custom_call_target="tpu_custom_call" | custom-call | tf_op jit(solution)/shard_map/mixer/pallas_call | solution.py:631
  33.1 0.7 %finish.1 = (bf16[32,2048]{1,0:T(8,128)(2,1)}, f32[2,256]{1,0:T(2,128)}) custom-call(bf16[32,2048]{1,0:T(8,128)(2,1)S(1)} %get-tuple-element.6.mixed_v, f32[2,256]{1,0:T(2,128)S(1)} %get-tuple-element.7.lse_v), custom_call_target="tpu_custom_call" | custom-call | tf_op jit(solution)/shard_map/finish/pallas_call | solution.py:696

commit v6 on v5

--- a/solution.py
+++ b/solution.py
@@ -413,21 +413,21 @@
             arrive(through, h, jj)
             send(through, h, jj, 3 * RING + y)
 
-    def attend_rows(backs):
+    def attend_group(places):
         for at in range(RING):
-            rows = [b for b in backs if b <= at]
-
-            @pl.when((z == at) & (y > 0) if rows == [0] else z == at)
+            here = [p for p in places if p[0] <= at]
+
+            @pl.when((z == at) & (y > 0) if all(b == 0 for b, _ in here) else z == at)
             def _():
-                blocks, shown = [], []
-                for b in rows:
-                    for up in (1, 2, 3) if b == 0 else (0, 1, 3, 2):
-                        blocks.append(shard_of(b, up))
-                        shown.append(y + up >= RING if b == 0 else None)
-                    if b > 0:
-                        gate_rows((z + RING - b) % RING, b).wait_recv()
-                if blocks:
-                    attend(blocks, shown=shown)
+                for back in dict.fromkeys(b for b, _ in here):
+                    if back and back not in gated[at]:
+                        gated[at].add(back)
+                        gate_rows((z + RING - back) % RING, back).wait_recv()
+                if here:
+                    shown = [y + up >= RING if back == 0 else None for back, up in here]
+                    attend([shard_of(*p) for p in here], shown=shown)
+
+    gated = [set() for _ in range(RING)]
 
     def read_state(ref, j):
         tail = ref[j, LANES:].astype(F32)
@@ -483,7 +483,7 @@
         both = jnp.concatenate([act_r[core], peer_r[...]], axis=1)
         for c in range(CHUNKS):
             cols = slice(c * CHUNK, (c + 1) * CHUNK)
-            product_v[:, cols] = dot(both, wor[:, cols])
+            product_v[:, cols] = dot(both, wor[:, cols]) + dot(act_a[core], woa[:LANES, cols])
 
     def handle_all(events):
         for h, back, up in events:
@@ -497,18 +497,15 @@
             start(z + k < RING, gate_rows(z, k))
 
     first_y()
+    first_z()
+    local = recurrence()
     last_y()
     share_row_gates()
-    first_z()
-    local = recurrence()
     share_states()
     last_z()
-    handle_all((
-        (1, 3, 0), (1, 1, 0), (0, 0, 3), (0, 0, 1),
-    ))
     query_side(*local)
     handle_all((
-        (0, 3, 0), (1, 2, 0), (1, 0, 1), (0, 1, 0),
+        (1, 3, 0), (1, 1, 0), (0, 0, 3), (0, 0, 1), (0, 3, 0), (1, 2, 0), (1, 0, 1), (0, 1, 0),
     ))
     share_weights()
     handle_all((
@@ -526,20 +523,20 @@
     handle_all((
         (1, 3, 1), (1, 1, 1), (0, 2, 0), (1, 2, 3), (1, 2, 1), (0, 1, 2), (1, 0, 2),
     ))
-    attend_rows((0,))
+    attend_group(((0, 1), (0, 2), (0, 3)))
     handle_all((
         (0, 1, 1), (0, 3, 2), (1, 3, 2),
     ))
-    attend_rows((3,))
+    attend_group(((3, 0), (3, 1), (3, 3), (3, 2)))
     handle_all((
         (1, 1, 2),
     ))
-    attend_rows((1,))
+    attend_group(((1, 0), (1, 1), (1, 3), (1, 2)))
     share_recurrence()
     handle_all((
         (1, 2, 2), (0, 2, 3), (0, 2, 1), (0, 2, 2),
     ))
-    attend_rows((2,))
+    attend_group(((2, 0), (2, 1), (2, 3), (2, 2)))
 
     a0, a1 = acc_v[0], acc_v[1]
     totals = jnp.where(low, a0, a1)
@@ -549,9 +546,6 @@
     by_owner(act_a, attn_out)
     act_copy = to_peer(3, act_a.at[1 - core], peer_a)
     start(None, act_copy)
-    log_sum = (jnp.where(low, m_v[0], m_v[1]) + jnp.log(totals)).T
-    lse_ref[0:1, :] = log_sum[0:1, :] + gates[sp, 0:1, :]
-    lse_ref[1:2, :] = log_sum[HALF : HALF + 1, :] + gates[sp, 1:2, :]
     await_entry(xc < 3, 2, 1)
     await_entry(xc == 0, 2, 3)
     project_recurrence()
@@ -576,15 +570,18 @@
     def summed(c):
         return x_copy(2, c, xsum.at[c], relayed.at[c], 2 * sides[c % 2] + core)
 
-    both = jnp.concatenate([act_a[core], peer_a[...]], axis=1)
+    theirs = peer_a[...]
     for c in range(CHUNKS):
         cols = slice(c * CHUNK, (c + 1) * CHUNK)
-        product = product_v[:, cols] + dot(both, woa[:, cols])
+        product = product_v[:, cols] + dot(theirs, woa[LANES:, cols])
         for b in range(RING):
             part[c, b] = product[32 * b : 32 * b + 32].astype(BF16)
         start(None, transit(c))
     for c in range(CHUNKS):
         start(None, direct(c))
+    log_sum = (jnp.where(low, m_v[0], m_v[1]) + jnp.log(totals)).T
+    lse_ref[0:1, :] = log_sum[0:1, :] + gates[sp, 0:1, :]
+    lse_ref[1:2, :] = log_sum[HALF : HALF + 1, :] + gates[sp, 1:2, :]
     for c in range(CHUNKS):
         transit(c).wait_recv()
         xsum[c] = (xt[c].astype(F32) + part[c, sides[c % 2]].astype(F32)).astype(BF16)

time: 34.3 us -> 34.2 us (level)
  no operation moved by 1% of the time
where the time goes in v6:
time: 34.2 us; the launch traced here: 33.8 us
  Pallas kernels  33 us (96%)
  between operations  0.81 us (2%)
    pallas_call x1, Pallas kernels, body(): pl.pallas_call(kernel, name='mixer', out_shape=(pltpu.VMEM((ROWS // 8, WI...  32.3 us

profile of v6, /device:TPU:97, one launch (start us, length us, event | category | flops | bytes accessed | tf_op | source)
XLA Modules:
  0.0 33.8 jit_solution(5041334143513263986)
XLA Ops:
  0.6 32.3 %mixer.1 = (bf16[32,2048]{1,0:T(8,128)(2,1)S(1)}, f32[2,256]{1,0:T(2,128)S(1)}) custom-call(bf16[256,2048]{1,0:T(8,128)(2,1)} %x_hbm.1, f32[1,2048]{1,0:T(1,128)} %bitcast.9, bf16[2048,128]{1,0:T(8,128)(2,1)} %wq_hbm.1, bf16[2048,128]{1,0:T(8,128)(2,1)} %wk_hbm.1, bf16[2048,128]{1,0:T(8,128)(2,1)} %wv_hbm.1, f32[1,64]{1,0:T(1,128)} %bitcast.12, ...), custom_call_target="tpu_custom_call" | custom-call | tf_op jit(solution)/shard_map/mixer/pallas_call | solution.py:628
  33.0 0.7 %finish.1 = (bf16[32,2048]{1,0:T(8,128)(2,1)}, f32[2,256]{1,0:T(2,128)}) custom-call(bf16[32,2048]{1,0:T(8,128)(2,1)S(1)} %get-tuple-element.6.mixed_v, f32[2,256]{1,0:T(2,128)S(1)} %get-tuple-element.7.lse_v), custom_call_target="tpu_custom_call" | custom-call | tf_op jit(solution)/shard_map/finish/pallas_call | solution.py:693

commit v7 on v6

--- a/solution.py
+++ b/solution.py
@@ -414,20 +414,22 @@
             send(through, h, jj, 3 * RING + y)
 
     def attend_group(places):
+        kinds = {}
         for at in range(RING):
-            here = [p for p in places if p[0] <= at]
-
-            @pl.when((z == at) & (y > 0) if all(b == 0 for b, _ in here) else z == at)
+            kinds.setdefault(tuple(p for p in places if p[0] <= at), []).append(at)
+        for here, zs in kinds.items():
+            at = zs[0]
+            inside = (z >= at) & (z <= zs[-1])
+
+            @pl.when(inside & (y > 0) if all(b == 0 for b, _ in here) else inside)
             def _():
                 for back in dict.fromkeys(b for b, _ in here):
-                    if back and back not in gated[at]:
-                        gated[at].add(back)
+                    if back:
                         gate_rows((z + RING - back) % RING, back).wait_recv()
                 if here:
                     shown = [y + up >= RING if back == 0 else None for back, up in here]
                     attend([shard_of(*p) for p in here], shown=shown)
 
-    gated = [set() for _ in range(RING)]
 
     def read_state(ref, j):
         tail = ref[j, LANES:].astype(F32)

time: 34.2 us -> 34 us (level)
  no operation moved by 1% of the time
where the time goes in v7:
time: 34 us; the launch traced here: 33.6 us
  Pallas kernels  32.9 us (97%)
  between operations  0.65 us (2%)
    pallas_call x1, Pallas kernels, body(): pl.pallas_call(kernel, name='mixer', out_shape=(pltpu.VMEM((ROWS // 8, WI...  32.2 us

profile of v7, /device:TPU:97, one launch (start us, length us, event | category | flops | bytes accessed | tf_op | source)
XLA Modules:
  0.0 33.6 jit_solution(13188307132059324625)
XLA Ops:
  0.6 32.2 %mixer.1 = (bf16[32,2048]{1,0:T(8,128)(2,1)S(1)}, f32[2,256]{1,0:T(2,128)S(1)}) custom-call(bf16[256,2048]{1,0:T(8,128)(2,1)} %x_hbm.1, f32[1,2048]{1,0:T(1,128)} %bitcast.9, bf16[2048,128]{1,0:T(8,128)(2,1)} %wq_hbm.1, bf16[2048,128]{1,0:T(8,128)(2,1)} %wk_hbm.1, bf16[2048,128]{1,0:T(8,128)(2,1)} %wv_hbm.1, f32[1,64]{1,0:T(1,128)} %bitcast.12, ...), custom_call_target="tpu_custom_call" | custom-call | tf_op jit(solution)/shard_map/mixer/pallas_call | solution.py:630
  32.9 0.7 %finish.1 = (bf16[32,2048]{1,0:T(8,128)(2,1)}, f32[2,256]{1,0:T(2,128)}) custom-call(bf16[32,2048]{1,0:T(8,128)(2,1)S(1)} %get-tuple-element.6.mixed_v, f32[2,256]{1,0:T(2,128)S(1)} %get-tuple-element.7.lse_v), custom_call_target="tpu_custom_call" | custom-call | tf_op jit(solution)/shard_map/finish/pallas_call | solution.py:695
